TPU v7x, 256 devices: a whole 4x4x8 slice. The times are simulated.
256 devices in a mesh: sp: 64 (over z, y, core), tp: 4 (over x).
Axes of the slice: x: 4, y: 4, z: 8, core: 2. Of those that a mesh axis runs over, the one named last changes fastest.
Arguments:
- residual: bfloat16 [4, 6144, 2048], P('tp', 'sp'), may hold values from -3 to 3
- query_nope: bfloat16 [4, 6144, 1024], P('tp', 'sp'), may hold values from -9 to 9
- query_rope: bfloat16 [4, 6144, 512], P('tp', 'sp'), may hold values from -48 to 48
- latent: bfloat16 [4, 6144, 128], P('tp', 'sp'), may hold values from -6 to 6
- rope_key: bfloat16 [4, 6144, 32], P('tp', 'sp'), may hold values from -48 to 48
- latent_gain: float32 [128], replicated, may hold values from 0.1 to 1.9
- up_key: bfloat16 [128, 1024], replicated, may hold values from -1 to 1
- up_value: bfloat16 [128, 1024], replicated, may hold values from -0.5 to 0.5
- out_weight: bfloat16 [1024, 2048], replicated, may hold values from -0.375 to 0.375
- ffn_gain: float32 [2048], replicated, may hold values from 0.1 to 1.9
- routes: int32 [4, 6144, 2], P(None, 'sp'), may hold values from 0 to 63, all different within a row; in each aligned block of 96 rows (0 to 95, 96 to 191, ..., all dimensions but the last counted through in order) at most 3 rows name the same one
- route_weight: float32 [4, 6144, 2], P('tp', 'sp'), may hold values from 0.1 to 1
- gate_weight: bfloat16 [64, 2048, 1024], P('sp', None, 'tp'), may hold values from -1.5 to 1.5
- up_weight: bfloat16 [64, 2048, 1024], P('sp', None, 'tp'), may hold values from -1.5 to 1.5
- down_weight: bfloat16 [64, 1024, 2048], P('sp', 'tp'), may hold values from -0.046875 to 0.046875
Outputs:
- updated: bfloat16 [4, 6144, 2048], P('tp', 'sp')
Inputs may be any that keep to these rules, and one draw needn't show every extreme that they name: `routes`: each row names 2 different experts. In each aligned block of 96 rows (one sequence's rows of one device) no expert is named by more than 3 rows, a bound that some block reaches.
All inputs are finite; a program needn't handle non-finite values.
Results may differ from a plain program's by a relative error of at most 0.017.
Values may be sent and summed in bfloat16 or wider, within the bound.
A program may use at most 64 MiB of HBM per device.

v0:
```python
import math

import jax
import jax.numpy as jnp
from jax import lax
from jax.sharding import Mesh
from jax.sharding import PartitionSpec as P

HEADS = 16
NOPE = 64
ROPE = 32
VDIM = 64
LATENT = 128
TOPK = 2
SP = ("sp_0", "sp_1", "sp_2")


EPS = 1e-06
ROPE_BASE = 10000.0
CLAMP = 7.0
ALPHA = 1.702
NEG_BIG = -1e30


def gather_axes(x, axes, dim):
    if not axes:
        return x
    nearer = lax.all_gather(x, axes[-1], axis=dim, tiled=True)
    return gather_axes(nearer, axes[:-1], dim)


def laid_out(pieces, dim):
    pieces = jnp.moveaxis(pieces, 0, dim)
    shape = pieces.shape
    return pieces.reshape(*shape[:dim], shape[dim] * shape[dim + 1], *shape[dim + 2 :])


def on_gathered_pieces(x, axis, dim, work, out_dim):
    width = x.shape[dim]
    pieces = jnp.split(x, 2, axis=dim) if width % 2 == 0 else [x]
    initial = jnp.arange(lax.axis_size(axis)) * width
    blocks = [lax.all_gather(section, axis) for section in pieces]
    made = [jax.vmap(work)(b, initial + k * (width // len(pieces))) for k, b in enumerate(blocks)]
    return laid_out(jnp.concatenate(made, axis=out_dim + 1), out_dim)


def split_up(x, dim, size):
    before, after = (x.shape[:dim], x.shape[dim + 1 :])
    return jnp.moveaxis(x.reshape(*before, size, -1, *after), dim, 0)


def sent_and_summed(x, axis, dim):
    size = lax.axis_size(axis)
    pieces = lax.all_to_all(split_up(x, dim, size), axis, 0, 0, tiled=True)
    return jnp.sum(pieces.astype(jnp.float32), axis=0)


def rotate(values, positions, width):
    half = width // 2
    inverse = ROPE_BASE ** (-jnp.arange(half, dtype=jnp.float32) * 2.0 / width)
    angle = positions.astype(jnp.float32)[:, None] * inverse[None, :]
    cosine = jnp.cos(angle)[:, None, :]
    sine = jnp.sin(angle)[:, None, :]
    first = values[..., :half]
    second = values[..., half:]
    return jnp.concatenate(
        [first * cosine - second * sine, first * sine + second * cosine], axis=-1
    )


def rms_scaled(values, gain):
    return values * lax.rsqrt(jnp.mean(values * values, axis=-1, keepdims=True) + EPS) * gain


def block_rows(rows):
    return math.gcd(rows, 512)


def expert_term(rows, gate_w, up_w, down_w):
    gate = jnp.minimum(jnp.dot(rows, gate_w, preferred_element_type=jnp.float32), CLAMP)
    lift = jnp.clip(jnp.dot(rows, up_w, preferred_element_type=jnp.float32), -CLAMP, CLAMP)
    active = (gate * jax.nn.sigmoid(ALPHA * gate) * (lift + 1.0)).astype(jnp.bfloat16)
    return jnp.dot(active, down_w, preferred_element_type=jnp.float32)


def assign(picks, slots, count):
    flat = picks.reshape(-1)
    hot = (flat[:, None] == jnp.arange(count, dtype=jnp.int32)[None, :]).astype(jnp.int32)
    ranks = jnp.sum((jnp.cumsum(hot, axis=0) - 1) * hot, axis=1)
    return flat * slots + ranks


def pack_rows(rows, target, slots, count):
    tokens = rows.shape[0]
    owner = jnp.arange(target.shape[0], dtype=jnp.int32) // (target.shape[0] // tokens)
    source = jnp.full((count * slots,), tokens, jnp.int32).at[target].set(owner)
    padded = jnp.concatenate([rows, jnp.zeros((1, rows.shape[1]), rows.dtype)], axis=0)
    return padded[source]


def local(
    residual,
    query_nope,
    query_rope,
    latent,
    rope_key,
    latent_gain,
    up_key,
    up_value,
    out_weight,
    ffn_gain,
    routes,
    route_weight,
    gate_weight,
    up_weight,
    down_weight,
):
    tokens = residual.shape[1]
    width = residual.shape[2]
    experts = lax.axis_size(SP)
    slots = min(tokens, max(2, 5 * tokens * TOPK // (4 * experts)))
    positions = lax.axis_index(SP) * tokens + jnp.arange(tokens, dtype=jnp.int32)
    factor = (NOPE + ROPE) ** (-0.5)
    normed = rms_scaled(latent[0].astype(jnp.float32), latent_gain).astype(jnp.bfloat16)
    key_turned = rotate(rope_key[0].astype(jnp.float32)[:, None, :], positions, ROPE)[
        :, 0, :
    ].astype(jnp.bfloat16)
    query_plain = query_nope[0].reshape(tokens, HEADS, NOPE)
    query_turned = rotate(
        query_rope[0].astype(jnp.float32).reshape(tokens, HEADS, ROPE), positions, ROPE
    ).astype(jnp.bfloat16)
    initial = (
        jnp.full((HEADS, tokens), NEG_BIG, jnp.float32),
        jnp.zeros((HEADS, tokens), jnp.float32),
        jnp.zeros((tokens, HEADS, VDIM), jnp.float32),
    )
    carry = initial
    piece = (
        gather_axes(normed, ("sp_2", "sp_0", "sp_1"), 0),
        gather_axes(key_turned, ("sp_2", "sp_0", "sp_1"), 0),
    )
    rows = piece[0].shape[0]
    span = block_rows(rows)
    latent_blocks = piece[0].reshape(rows // span, span, LATENT)
    turned_blocks = piece[1].reshape(rows // span, span, ROPE)

    def step(state, blocks):
        peak_old, total, summed = state
        keys = jnp.dot(blocks[0], up_key, preferred_element_type=jnp.float32).astype(jnp.bfloat16)
        keys = keys.reshape(span, HEADS, NOPE)
        values = jnp.dot(blocks[0], up_value, preferred_element_type=jnp.float32).astype(
            jnp.bfloat16
        )
        values = values.reshape(span, HEADS, VDIM)
        scores = (
            jnp.einsum("qhd,khd->hqk", query_plain, keys, preferred_element_type=jnp.float32)
            + jnp.einsum("qhd,kd->hqk", query_turned, blocks[1], preferred_element_type=jnp.float32)
        ) * factor
        peak = jnp.maximum(peak_old, jnp.max(scores, axis=-1))
        shrink = jnp.exp(peak_old - peak)
        weights = jnp.exp(scores - peak[:, :, None])
        total = total * shrink + jnp.sum(weights, axis=-1)
        mixed = jnp.einsum(
            "hqk,khd->qhd", weights.astype(jnp.bfloat16), values, preferred_element_type=jnp.float32
        )
        summed = summed * jnp.transpose(shrink)[:, :, None] + mixed
        return ((peak, total, summed), None)

    carry, _ = lax.scan(step, carry, (latent_blocks, turned_blocks))
    peak, total, summed = carry
    attended = (
        (summed / jnp.transpose(total)[:, :, None])
        .reshape(tokens, HEADS * VDIM)
        .astype(jnp.bfloat16)
    )
    projected = jnp.dot(attended, out_weight, preferred_element_type=jnp.float32)
    middle = (residual[0].astype(jnp.float32) + projected).astype(jnp.bfloat16)
    middle_wide = middle.astype(jnp.float32)
    normal_rows = rms_scaled(middle_wide, ffn_gain).astype(jnp.bfloat16)
    own_picks = lax.dynamic_index_in_dim(routes, lax.axis_index("tp"), 0, keepdims=False)
    own_target = assign(own_picks, slots, experts)
    outgoing = pack_rows(normal_rows, own_target, slots, experts).reshape(1, experts, slots, width)
    arrived = lax.all_to_all(outgoing, SP, split_axis=1, concat_axis=1, tiled=True)

    def partial_rows(piece, start):
        return expert_term(piece.reshape(-1, width), gate_weight[0], up_weight[0], down_weight[0])

    terms = on_gathered_pieces(arrived, "tp", 0, partial_rows, 0)
    mine = sent_and_summed(terms.astype(jnp.bfloat16), "tp", 0)
    returned = lax.all_to_all(
        mine.astype(jnp.bfloat16).reshape(1, experts, slots, width),
        SP,
        split_axis=1,
        concat_axis=1,
        tiled=True,
    )
    picked = returned.reshape(experts * slots, width)[own_target].reshape(tokens, TOPK, width)
    combined = jnp.sum(picked.astype(jnp.float32) * route_weight[0][:, :, None], axis=1)
    return (middle_wide + combined).astype(jnp.bfloat16)[None]


def solution(mesh):
    split = Mesh(mesh.devices.reshape(8, 4, 2, mesh.shape["tp"]), ("sp_0", "sp_1", "sp_2", "tp"))
    in_specs = (
        P("tp", SP, None),
        P("tp", SP, None),
        P("tp", SP, None),
        P("tp", SP, None),
        P("tp", SP, None),
        P(),
        P(),
        P(),
        P(),
        P(),
        P(None, SP, None),
        P("tp", SP, None),
        P(SP, None, "tp"),
        P(SP, None, "tp"),
        P(SP, "tp", None),
    )
    out_specs = P("tp", SP, None)
    return jax.shard_map(local, mesh=split, in_specs=in_specs, out_specs=out_specs, check_vma=False)
```

profile of v0, /device:TPU:1, one launch (start us, length us, event | category | flops | bytes accessed | tf_op | source)
XLA Modules:
  0.0 452.2 jit_solution(16603405497418212212)
XLA Ops:
  8.3 10.5 %all_gather.24 = bf16[384,128]{1,0:T(8,128)(2,1)S(1)} all-gather(bf16[96,128]{1,0:T(8,128)(2,1)S(1)} %fusion.52), channel_id=1, replica_groups=mesh['sp_0'=8,'sp_1'=4,'sp_2'=2,'tp'=4] {'sp_1'}, dimensions={0}, use_global_device_ids=true | all-gather | bytes 122880 | tf_op jit(solution)/shard_map/all_gather | solution.py:28
  18.8 25.6 %all_gather.25 = bf16[3072,128]{1,0:T(8,128)(2,1)} all-gather(bf16[384,128]{1,0:T(8,128)(2,1)S(1)} %all_gather.24), channel_id=1, replica_groups=mesh['sp_0'=8,'sp_1'=4,'sp_2'=2,'tp'=4] {'sp_0'}, dimensions={0}, use_global_device_ids=true | all-gather | bytes 884736 | tf_op jit(solution)/shard_map/all_gather | solution.py:28
  46.5 9.6 %all-gather = bf16[384,1,32]{2,1,0:T(2,128)(2,1)S(1)} all-gather(bf16[96,1,32]{2,1,0:T(2,128)(2,1)S(1)} %copy.55), channel_id=2, replica_groups=mesh['sp_0'=8,'sp_1'=4,'sp_2'=2,'tp'=4] {'sp_1'}, dimensions={0}, use_global_device_ids=true | all-gather | bytes 30720 | tf_op jit(solution)/shard_map/all_gather | solution.py:28
  56.2 18.6 %all-gather.1 = bf16[3072,1,32]{0,2,1:T(8,128)(2,1)S(1)} all-gather(bf16[384,1,32]{0,2,1:T(8,128)(2,1)S(1)} %copy.56), channel_id=3, replica_groups=mesh['sp_0'=8,'sp_1'=4,'sp_2'=2,'tp'=4] {'sp_0'}, dimensions={0}, use_global_device_ids=true | all-gather | bytes 221184 | tf_op jit(solution)/shard_map/all_gather | solution.py:28
  74.8 20.0 %all-gather.2 = bf16[6144,1,32]{0,2,1:T(8,128)(2,1)S(1)} all-gather(bf16[3072,1,32]{0,2,1:T(8,128)(2,1)S(1)} %all-gather.1), channel_id=4, replica_groups=mesh['sp_0'=8,'sp_1'=4,'sp_2'=2,'tp'=4] {'sp_2'}, dimensions={0}, use_global_device_ids=true | all-gather | bytes 589824 | tf_op jit(solution)/shard_map/all_gather | solution.py:28
  100.5 154.8 %while.15 = (s32[]{:T(128)}, f32[16,96]{1,0:T(8,128)}, f32[16,96]{1,0:T(8,128)}, f32[96,16,64]{0,2,1:T(8,128)}, bf16[12,512,128]{2,1,0:T(8,128)(2,1)}, /*index=5...) while((s32[]{:T(128)}, f32[16,96]{1,0:T(8,128)}, ...), condition=%wide.region_4.5_spmd.clone, body=%wide.region_1.4_spmd.clone.sunk | while | flops 526951424 | bytes 40896332 | solution.py:169
  103.0 3.1 fusion.99
  108.1 3.7 fusion.103
  115.9 3.1 fusion.99
  120.9 3.7 fusion.103
  128.8 3.1 fusion.99
  133.8 3.7 fusion.103
  141.7 3.1 fusion.99
  146.7 3.7 fusion.103
  159.6 3.7 fusion.103
  172.5 3.7 fusion.103
  185.4 3.7 fusion.103
  198.3 3.7 fusion.103
  211.2 3.7 fusion.103
  224.2 3.7 fusion.103
  237.1 3.7 fusion.103
  250.0 3.7 fusion.103
  256.5 3.2 multiply_reduce_fusion.1
  262.5 35.7 %all_to_all.15 = bf16[1,64,3,2048]{3,2,0,1:T(4,128)(2,1)S(1)} all-to-all(bf16[1,64,3,2048]{3,2,0,1:T(4,128)(2,1)} %bitcast.117), channel_id=1, replica_groups=mesh['sp_0'=8,'sp_1'=4,'sp_2'=2,'tp'=4] {'sp_0','sp_1','sp_2'}, dimensions={1} | all-to-all | bytes 1572864 | tf_op jit(solution)/shard_map/all_to_all | solution.py:183
  299.7 38.9 %all-gather.9.cloned.1.call-done = bf16[4,64,3,2048]{3,1,2,0:T(8,128)(2,1)} async-done(((bf16[1,64,3,2048]{3,1,2,0:T(8,128)(2,1)}), bf16[4,64,3,2048]{3,1,2,0:T(8,128)(2,1)}) %all-gather.9.cloned.1.call-update) | async-done | bytes 3145744 | tf_op jit(solution)/shard_map/all_gather | solution.py:42
  338.6 4.4 copy.65
  343.0 3.4 fusion.29
  346.5 3.6 fusion.41
  351.1 39.9 %all_to_all.16 = bf16[4,192,2048]{2,1,0:T(8,128)(2,1)} all-to-all(bf16[4,192,2048]{2,1,0:T(8,128)(2,1)S(1)} %bitcast.114), channel_id=1, replica_groups=mesh['sp_0'=8,'sp_1'=4,'sp_2'=2,'tp'=4] {'tp'}, dimensions={0} | all-to-all | bytes 6291456 | tf_op jit(solution)/shard_map/all_to_all | solution.py:54
  394.9 12.1 %all-to-all-start.2 = ((bf16[1,64,3,2048]{3,2,0,1:T(4,128)(2,1)}), bf16[1,64,3,2048]{3,2,0,1:T(4,128)(2,1)}, u32[]{:S(2)}, u32[]{:S(2)}) async-start(bf16[1,64,3,2048]{3,2,0,1:T(4,128)(2,1)} %bitcast.116), calls=%async_computation.2 | async-start | bytes 2097152 | tf_op jit(solution)/shard_map/all_to_all | solution.py:190
  407.1 28.0 %all-to-all-done.2 = bf16[1,64,3,2048]{3,2,0,1:T(4,128)(2,1)} async-done(((bf16[1,64,3,2048]{3,2,0,1:T(4,128)(2,1)}), bf16[1,64,3,2048]{3,2,0,1:T(4,128)(2,1)}, u32[]{:S(2)}, u32[]{:S(2)}) %all-to-all-start.2) | async-done | bytes 786464 | tf_op jit(solution)/shard_map/all_to_all | solution.py:190
  440.8 3.7 multiply_reduce_fusion
  (361 shorter events, 122.6 us)
Async XLA Ops:
  6.5 343.5 %copy-start = (bf16[1,256,2048]{2,1,0:T(8,128)(2,1)S(1)}, bf16[1,256,2048]{2,1,0:T(8,128)(2,1)}, u32[]{:S(2)}) copy-start(bf16[1,256,2048]{2,1,0:T(8,128)(2,1)} %param.31) | copy-start | bytes 3145732
  6.5 89.5 %copy-start.9 = (bf16[1,96,1024]{2,1,0:T(8,128)(2,1)S(1)}, bf16[1,96,1024]{2,1,0:T(8,128)(2,1)}, u32[]{:S(2)}) copy-start(bf16[1,96,1024]{2,1,0:T(8,128)(2,1)} %param.18) | copy-start | bytes 589828
  6.5 94.0 %all-gather.7.cloned.1.call-start = ((), (), s32[]{:S(2)}) async-start(), calls=%async_computation.3 | async-start | bytes 2359296 | tf_op jit(solution)/shard_map/all_gather | solution.py:28
  44.4 56.1 %copy-start.2 = (bf16[128,1024]{1,0:T(8,128)(2,1)S(1)}, bf16[128,1024]{1,0:T(8,128)(2,1)}, u32[]{:S(2)}) copy-start(bf16[128,1024]{1,0:T(8,128)(2,1)} %param.23) | copy-start | bytes 786436
  44.4 294.2 %all-gather.9.cloned.1.call-start = ((), (), s32[]{:S(2)}) async-start(), calls=%async_computation.4 | async-start | bytes 3932160 | tf_op jit(solution)/shard_map/all_gather | solution.py:42
  108.0 4.7 %copy-start.6 = (f32[16,96]{1,0:T(8,128)S(1)}, f32[16,96]{1,0:T(8,128)}, u32[]{:S(2)}) copy-start(f32[16,96]{1,0:T(8,128)} %get-tuple-element.239) | copy-start | bytes 18436 | tf_op jit(solution)/shard_map/while
  108.0 4.7 %copy-start.7 = (f32[16,96]{1,0:T(8,128)S(1)}, f32[16,96]{1,0:T(8,128)}, u32[]{:S(2)}) copy-start(f32[16,96]{1,0:T(8,128)} %get-tuple-element.240) | copy-start | bytes 18436 | tf_op jit(solution)/shard_map/while
  120.9 4.7 %copy-start.6 = (f32[16,96]{1,0:T(8,128)S(1)}, f32[16,96]{1,0:T(8,128)}, u32[]{:S(2)}) copy-start(f32[16,96]{1,0:T(8,128)} %get-tuple-element.239) | copy-start | bytes 18436 | tf_op jit(solution)/shard_map/while
  120.9 4.7 %copy-start.7 = (f32[16,96]{1,0:T(8,128)S(1)}, f32[16,96]{1,0:T(8,128)}, u32[]{:S(2)}) copy-start(f32[16,96]{1,0:T(8,128)} %get-tuple-element.240) | copy-start | bytes 18436 | tf_op jit(solution)/shard_map/while
  133.8 4.7 %copy-start.6 = (f32[16,96]{1,0:T(8,128)S(1)}, f32[16,96]{1,0:T(8,128)}, u32[]{:S(2)}) copy-start(f32[16,96]{1,0:T(8,128)} %get-tuple-element.239) | copy-start | bytes 18436 | tf_op jit(solution)/shard_map/while
  133.8 4.7 %copy-start.7 = (f32[16,96]{1,0:T(8,128)S(1)}, f32[16,96]{1,0:T(8,128)}, u32[]{:S(2)}) copy-start(f32[16,96]{1,0:T(8,128)} %get-tuple-element.240) | copy-start | bytes 18436 | tf_op jit(solution)/shard_map/while
  146.7 4.7 %copy-start.6 = (f32[16,96]{1,0:T(8,128)S(1)}, f32[16,96]{1,0:T(8,128)}, u32[]{:S(2)}) copy-start(f32[16,96]{1,0:T(8,128)} %get-tuple-element.239) | copy-start | bytes 18436 | tf_op jit(solution)/shard_map/while
  146.7 4.7 %copy-start.7 = (f32[16,96]{1,0:T(8,128)S(1)}, f32[16,96]{1,0:T(8,128)}, u32[]{:S(2)}) copy-start(f32[16,96]{1,0:T(8,128)} %get-tuple-element.240) | copy-start | bytes 18436 | tf_op jit(solution)/shard_map/while
  159.6 4.7 %copy-start.6 = (f32[16,96]{1,0:T(8,128)S(1)}, f32[16,96]{1,0:T(8,128)}, u32[]{:S(2)}) copy-start(f32[16,96]{1,0:T(8,128)} %get-tuple-element.239) | copy-start | bytes 18436 | tf_op jit(solution)/shard_map/while
  159.6 4.7 %copy-start.7 = (f32[16,96]{1,0:T(8,128)S(1)}, f32[16,96]{1,0:T(8,128)}, u32[]{:S(2)}) copy-start(f32[16,96]{1,0:T(8,128)} %get-tuple-element.240) | copy-start | bytes 18436 | tf_op jit(solution)/shard_map/while
  172.5 4.7 %copy-start.6 = (f32[16,96]{1,0:T(8,128)S(1)}, f32[16,96]{1,0:T(8,128)}, u32[]{:S(2)}) copy-start(f32[16,96]{1,0:T(8,128)} %get-tuple-element.239) | copy-start | bytes 18436 | tf_op jit(solution)/shard_map/while
  172.5 4.7 %copy-start.7 = (f32[16,96]{1,0:T(8,128)S(1)}, f32[16,96]{1,0:T(8,128)}, u32[]{:S(2)}) copy-start(f32[16,96]{1,0:T(8,128)} %get-tuple-element.240) | copy-start | bytes 18436 | tf_op jit(solution)/shard_map/while
  185.4 4.7 %copy-start.6 = (f32[16,96]{1,0:T(8,128)S(1)}, f32[16,96]{1,0:T(8,128)}, u32[]{:S(2)}) copy-start(f32[16,96]{1,0:T(8,128)} %get-tuple-element.239) | copy-start | bytes 18436 | tf_op jit(solution)/shard_map/while
  185.4 4.7 %copy-start.7 = (f32[16,96]{1,0:T(8,128)S(1)}, f32[16,96]{1,0:T(8,128)}, u32[]{:S(2)}) copy-start(f32[16,96]{1,0:T(8,128)} %get-tuple-element.240) | copy-start | bytes 18436 | tf_op jit(solution)/shard_map/while
  198.3 4.7 %copy-start.6 = (f32[16,96]{1,0:T(8,128)S(1)}, f32[16,96]{1,0:T(8,128)}, u32[]{:S(2)}) copy-start(f32[16,96]{1,0:T(8,128)} %get-tuple-element.239) | copy-start | bytes 18436 | tf_op jit(solution)/shard_map/while
  198.3 4.7 %copy-start.7 = (f32[16,96]{1,0:T(8,128)S(1)}, f32[16,96]{1,0:T(8,128)}, u32[]{:S(2)}) copy-start(f32[16,96]{1,0:T(8,128)} %get-tuple-element.240) | copy-start | bytes 18436 | tf_op jit(solution)/shard_map/while
  211.2 4.7 %copy-start.6 = (f32[16,96]{1,0:T(8,128)S(1)}, f32[16,96]{1,0:T(8,128)}, u32[]{:S(2)}) copy-start(f32[16,96]{1,0:T(8,128)} %get-tuple-element.239) | copy-start | bytes 18436 | tf_op jit(solution)/shard_map/while
  211.2 4.7 %copy-start.7 = (f32[16,96]{1,0:T(8,128)S(1)}, f32[16,96]{1,0:T(8,128)}, u32[]{:S(2)}) copy-start(f32[16,96]{1,0:T(8,128)} %get-tuple-element.240) | copy-start | bytes 18436 | tf_op jit(solution)/shard_map/while
  224.1 4.7 %copy-start.6 = (f32[16,96]{1,0:T(8,128)S(1)}, f32[16,96]{1,0:T(8,128)}, u32[]{:S(2)}) copy-start(f32[16,96]{1,0:T(8,128)} %get-tuple-element.239) | copy-start | bytes 18436 | tf_op jit(solution)/shard_map/while
  224.1 4.7 %copy-start.7 = (f32[16,96]{1,0:T(8,128)S(1)}, f32[16,96]{1,0:T(8,128)}, u32[]{:S(2)}) copy-start(f32[16,96]{1,0:T(8,128)} %get-tuple-element.240) | copy-start | bytes 18436 | tf_op jit(solution)/shard_map/while
  237.0 4.7 %copy-start.6 = (f32[16,96]{1,0:T(8,128)S(1)}, f32[16,96]{1,0:T(8,128)}, u32[]{:S(2)}) copy-start(f32[16,96]{1,0:T(8,128)} %get-tuple-element.239) | copy-start | bytes 18436 | tf_op jit(solution)/shard_map/while
  237.0 4.7 %copy-start.7 = (f32[16,96]{1,0:T(8,128)S(1)}, f32[16,96]{1,0:T(8,128)}, u32[]{:S(2)}) copy-start(f32[16,96]{1,0:T(8,128)} %get-tuple-element.240) | copy-start | bytes 18436 | tf_op jit(solution)/shard_map/while
  249.9 4.7 %copy-start.6 = (f32[16,96]{1,0:T(8,128)S(1)}, f32[16,96]{1,0:T(8,128)}, u32[]{:S(2)}) copy-start(f32[16,96]{1,0:T(8,128)} %get-tuple-element.239) | copy-start | bytes 18436 | tf_op jit(solution)/shard_map/while
  250.0 4.7 %copy-start.7 = (f32[16,96]{1,0:T(8,128)S(1)}, f32[16,96]{1,0:T(8,128)}, u32[]{:S(2)}) copy-start(f32[16,96]{1,0:T(8,128)} %get-tuple-element.240) | copy-start | bytes 18436 | tf_op jit(solution)/shard_map/while
  391.0 16.0 %copy-start.13 = (f32[1,96,2]{1,2,0:T(2,128)S(1)}, f32[1,96,2]{1,2,0:T(2,128)}, u32[]{:S(2)}) copy-start(f32[1,96,2]{1,2,0:T(2,128)} %param.28) | copy-start | bytes 2308
  391.0 16.1 %copy-start.12 = (s32[192,1]{0,1:T(1,128)S(1)}, s32[192,1]{0,1:T(1,128)}, u32[]{:S(2)}) copy-start(s32[192,1]{0,1:T(1,128)} %copy-done.11) | copy-start | bytes 2308
  394.9 40.2 %all-to-all-start.2 = ((bf16[1,64,3,2048]{3,2,0,1:T(4,128)(2,1)}), bf16[1,64,3,2048]{3,2,0,1:T(4,128)(2,1)}, u32[]{:S(2)}, u32[]{:S(2)}) async-start(bf16[1,64,3,2048]{3,2,0,1:T(4,128)(2,1)} %bitcast.116), calls=%async_computation.2 | async-start | bytes 2097152 | tf_op jit(solution)/shard_map/all_to_all | solution.py:190
  (64 other events, 160.5 us)
Sparse Core Ops, SparseCore 0:
  44.5 23.3 all-gather.6
  299.8 38.7 all-gather.8
where the time goes:
time: 453 us; the launch traced here: 452 us
  blocking collectives  160 us (35%)
  matrix products  132 us (29%)
  waiting for transfers between devices  66.9 us (15%)
  local copies, waits for them, and re-layouts  40.6 us (9%)
  other arithmetic  25.2 us (6%)
  between operations  13.8 us (3%)
  starting transfers between devices  12.2 us (3%)
    all_gather x5, blocking collectives, gather_axes(): nearer = lax.all_gather(x, axes[-1], axis=dim, tiled=True)  84.3 us
    dot_general x12, matrix products, step(): jnp.einsum('hqk,khd->qhd', weights.astype(jnp.bfloat16), values, preferre...  44.9 us
    all_to_all x1, blocking collectives, sent_and_summed(): pieces = lax.all_to_all(split_up(x, dim, size), axis, 0, 0, tiled=True)  39.9 us
    all_gather x1, waiting for transfers between devices, on_gathered_pieces(): blocks = [lax.all_gather(section, axis) for section in pieces]  38.9 us
    dot_general x12, matrix products, step(): jnp.einsum('qhd,kd->hqk', query_turned, blocks[1], preferred_element_type...  36.8 us
    all_to_all x1, blocking collectives, local(): lax.all_to_all(outgoing, SP, split_axis=1, concat_axis=1, tiled=True)  35.7 us
    all_to_all x1, waiting for transfers between devices, local(): lax.all_to_all(mine.astype(jnp.bfloat16).reshape(1, experts, slots, width...  28 us
    dot_general x12, matrix products, step(): jnp.dot(blocks[0], up_value, preferred_element_type=jnp.float32)  16 us
  transfers between devices with their start and end apart: 3, of which 2 were waited for; matrix products, arithmetic and copies ran while one was open for 2% of the time, Pallas kernels for 0%

commit v1 on v0

v1 whole, which is shorter than its diff:
```python
import math

import jax
import jax.numpy as jnp
from jax import lax
from jax.experimental import pallas as pl
from jax.experimental.pallas import tpu as pltpu
from jax.sharding import Mesh
from jax.sharding import PartitionSpec as P

HEADS = 16
NOPE = 64
ROPE = 32
VDIM = 64
LATENT = 128
TOPK = 2
SP = ("sp_0", "sp_1", "sp_2")

EPS = 1e-06
ROPE_BASE = 10000.0
CLAMP = 7.0
ALPHA = 1.702
NEG_BIG = -1e30
MESH = pl.DeviceIdType.MESH

F32 = jnp.float32
BF16 = jnp.bfloat16
NZ, NY = 8, 4
TOK = 96
GROUP = NZ * TOK
QROWS = HEADS * TOK
CHUNK = 512
VROWS = LATENT + 16
Z_ORDER = (1, 7, 2, 6, 3, 5, 4)


def gather_axes(x, axes, dim):
    if not axes:
        return x
    nearer = lax.all_gather(x, axes[-1], axis=dim, tiled=True)
    return gather_axes(nearer, axes[:-1], dim)


def laid_out(pieces, dim):
    pieces = jnp.moveaxis(pieces, 0, dim)
    shape = pieces.shape
    return pieces.reshape(*shape[:dim], shape[dim] * shape[dim + 1], *shape[dim + 2 :])


def on_gathered_pieces(x, axis, dim, work, out_dim):
    width = x.shape[dim]
    pieces = jnp.split(x, 2, axis=dim) if width % 2 == 0 else [x]
    initial = jnp.arange(lax.axis_size(axis)) * width
    blocks = [lax.all_gather(section, axis) for section in pieces]
    made = [jax.vmap(work)(b, initial + k * (width // len(pieces))) for k, b in enumerate(blocks)]
    return laid_out(jnp.concatenate(made, axis=out_dim + 1), out_dim)


def split_up(x, dim, size):
    before, after = (x.shape[:dim], x.shape[dim + 1 :])
    return jnp.moveaxis(x.reshape(*before, size, -1, *after), dim, 0)


def sent_and_summed(x, axis, dim):
    size = lax.axis_size(axis)
    pieces = lax.all_to_all(split_up(x, dim, size), axis, 0, 0, tiled=True)
    return jnp.sum(pieces.astype(jnp.float32), axis=0)


def expert_term(rows, gate_w, up_w, down_w):
    gate = jnp.minimum(jnp.dot(rows, gate_w, preferred_element_type=jnp.float32), CLAMP)
    lift = jnp.clip(jnp.dot(rows, up_w, preferred_element_type=jnp.float32), -CLAMP, CLAMP)
    active = (gate * jax.nn.sigmoid(ALPHA * gate) * (lift + 1.0)).astype(jnp.bfloat16)
    return jnp.dot(active, down_w, preferred_element_type=jnp.float32)


def assign(picks, slots, count):
    flat = picks.reshape(-1)
    hot = (flat[:, None] == jnp.arange(count, dtype=jnp.int32)[None, :]).astype(jnp.int32)
    ranks = jnp.sum((jnp.cumsum(hot, axis=0) - 1) * hot, axis=1)
    return flat * slots + ranks


def pack_rows(rows, target, slots, count):
    tokens = rows.shape[0]
    owner = jnp.arange(target.shape[0], dtype=jnp.int32) // (target.shape[0] // tokens)
    source = jnp.full((count * slots,), tokens, jnp.int32).at[target].set(owner)
    padded = jnp.concatenate([rows, jnp.zeros((1, rows.shape[1]), rows.dtype)], axis=0)
    return padded[source]


def nt_dot(a, b):
    return lax.dot_general(a, b, (((1,), (1,)), ((), ())), preferred_element_type=F32)


def iota(shape, dim):
    return lax.broadcasted_iota(jnp.int32, shape, dim)


def turned(x, cosine, sine):
    low = iota(x.shape, 1) % ROPE < ROPE // 2
    swapped = jnp.where(low, pltpu.roll(x, 128 - ROPE // 2, 1), pltpu.roll(x, ROPE // 2, 1))
    return x * cosine + swapped * sine


def attention_kernel(
    qn_ref, qr_ref, lat_ref, key_ref, cos_ref, sin_ref, gain_ref, upk_ref, upv_ref,
    res_ref, fgain_ref, ow_hbm,
    mid_ref, rows_ref,
    held, q_ref, k_ref, v_ref, s_ref, p_ref, acc_ref, peak_ref, ow_ref,
    own_send, fwd_send, pair_send, z_recv, y_recv, pair_recv, ow_sem,
):
    z, y, c = (lax.axis_index(name) for name in SP)
    barrier = pltpu.get_barrier_semaphore()

    def z_peer(d):
        return {"sp_0": lax.rem(z + d, NZ)}

    def y_peer(d):
        return {"sp_1": lax.rem(y + d, NY)}

    partner = {"sp_2": 1 - c}
    for d in range(1, NZ):
        pl.semaphore_signal(barrier, inc=1, device_id=z_peer(d), device_id_type=MESH)
    for d in range(1, NY):
        pl.semaphore_signal(barrier, inc=1, device_id=y_peer(d), device_id_type=MESH)
    pl.semaphore_signal(barrier, inc=1, device_id=partner, device_id_type=MESH)
    ow_copy = pltpu.make_async_copy(ow_hbm, ow_ref, ow_sem)
    ow_copy.start()

    wide = lat_ref[...].astype(F32)
    scale = lax.rsqrt(jnp.mean(wide * wide, axis=-1, keepdims=True) + EPS)
    held[c, y, z, :TOK, :] = (wide * scale * gain_ref[...]).astype(BF16)
    held[c, y, z, TOK:, :] = turned(
        key_ref[...].astype(F32), cos_ref[TOK:, :], sin_ref[TOK:, :]
    ).astype(BF16)

    pl.semaphore_wait(barrier, NZ + NY - 1)

    def to_y(block):
        for d in (1, 3, 2):
            pltpu.make_async_remote_copy(
                src_ref=block, dst_ref=block, send_sem=fwd_send, recv_sem=y_recv.at[y],
                device_id=y_peer(d), device_id_type=MESH,
            ).start()

    mine = held.at[c, y, z]
    for d in Z_ORDER:
        pltpu.make_async_remote_copy(
            src_ref=mine, dst_ref=mine, send_sem=own_send, recv_sem=z_recv.at[z],
            device_id=z_peer(d), device_id_type=MESH,
        ).start()
    to_y(mine)

    fold = (NOPE + ROPE) ** (-0.5) * math.log2(math.e)
    lane = iota((TOK, 128), 1)
    in_lane, out_lane = iota((128, 128), 0), iota((128, 128), 1)
    turned_tiles = []
    for t in range(HEADS * ROPE // 128):
        tile = qr_ref[:, 128 * t : 128 * t + 128].astype(F32)
        turned_tiles.append((turned(tile, cos_ref[:TOK, :], sin_ref[:TOK, :]) * fold).astype(BF16))
    pick = [
        jnp.where((out_lane < TOK) & (in_lane == ROPE * m + out_lane % ROPE), 1.0, 0.0).astype(BF16)
        for m in range(4)
    ]
    for h in range(HEADS):
        t = h // 2
        plain = qn_ref[:, 128 * t : 128 * t + 128]
        half = lane < NOPE if h % 2 == 0 else lane >= NOPE
        plain = jnp.where(half, plain, jnp.zeros_like(plain))
        lifted = nt_dot(plain, upk_ref[:, 128 * t : 128 * t + 128]) * fold
        q_ref[TOK * h : TOK * h + TOK, :128] = lifted.astype(BF16)
        rotary = jnp.dot(turned_tiles[h // 4], pick[h % 4], preferred_element_type=F32)
        q_ref[TOK * h : TOK * h + TOK, 128:] = rotary.astype(BF16)

    acc_ref[...] = jnp.zeros_like(acc_ref)
    peak_ref[...] = jnp.full_like(peak_ref, NEG_BIG)
    v_ref[LATENT:, :] = jnp.ones((VROWS - LATENT, GROUP), BF16)

    for d in Z_ORDER:
        source = lax.rem(z + d, NZ)
        block = held.at[c, y, source]
        pltpu.make_async_copy(block, block, z_recv.at[source]).wait()
        to_y(block)

    def step(s, _):
        k = lax.rem(s + 1, 3)
        dy = jnp.where(s < 2, 0, jnp.where(k == 0, 1, jnp.where(k == 1, 3, 2)))
        gy = lax.rem(y + dy, NY)
        own = (s == 0) | ((s >= 2) & (s <= 4))
        gc = jnp.where(own, c, 1 - c)
        group = held.at[gc, gy]

        @pl.when(own)
        def _():
            @pl.when(s > 0)
            def _():
                pltpu.make_async_copy(group, group, y_recv.at[gy]).wait()

            pltpu.make_async_remote_copy(
                src_ref=group, dst_ref=group, send_sem=pair_send.at[gy],
                recv_sem=pair_recv.at[gy], device_id=partner, device_id_type=MESH,
            ).start()

        @pl.when(jnp.logical_not(own))
        def _():
            pltpu.make_async_copy(group, group, pair_recv.at[gy]).wait()

        lane32 = iota((32, 128), 1) // ROPE
        for b in range(NZ):
            k_ref[TOK * b : TOK * b + TOK, :128] = held[gc, gy, b, :TOK, :]
            packed = held[gc, gy, b, TOK:, :]
            for j in range(TOK // 32):
                row = TOK * b + 32 * j
                k_ref[row : row + 32, 128:] = jnp.where(lane32 == j, packed, jnp.zeros_like(packed))
        for b in range(GROUP // 128):
            v_ref[:LATENT, 128 * b : 128 * b + 128] = k_ref[128 * b : 128 * b + 128, :128].T

        for n in range(QROWS // CHUNK):
            cols = slice(CHUNK * n, CHUNK * n + CHUNK)
            s_ref[n] = nt_dot(k_ref[...], q_ref[cols, :])
            old = peak_ref[:, cols]
            top = jnp.maximum(old, jnp.max(s_ref[n], axis=0, keepdims=True))
            shrink = jnp.exp2(old - top)
            peak_ref[:, cols] = top
            p_ref[n] = jnp.exp2(s_ref[n] - top).astype(BF16)
            mixed = jnp.dot(v_ref[...], p_ref[n], preferred_element_type=F32)
            acc_ref[:, cols] = acc_ref[:, cols] * shrink + mixed
        return 0

    lax.fori_loop(0, 2 * NY, step, 0)

    lat_t = acc_ref[:LATENT, :] / acc_ref[LATENT : LATENT + 1, :]
    mixed_rows = jnp.concatenate(
        [lat_t[:, 128 * b : 128 * b + 128].T for b in range(QROWS // 128)], axis=0
    ).astype(BF16)
    tiles = []
    for t in range(HEADS // 2):
        up = upv_ref[:, 128 * t : 128 * t + 128]
        even = jnp.dot(mixed_rows[192 * t : 192 * t + 96], up, preferred_element_type=F32)
        odd = jnp.dot(mixed_rows[192 * t + 96 : 192 * t + 192], up, preferred_element_type=F32)
        tiles.append(jnp.where(lane < VDIM, even, odd).astype(BF16))
    attended = jnp.concatenate(tiles, axis=1)
    ow_copy.wait()
    projected = jnp.dot(attended, ow_ref[...], preferred_element_type=F32)
    middle = (res_ref[...].astype(F32) + projected).astype(BF16)
    mid_ref[...] = middle
    wide = middle.astype(F32)
    scale = lax.rsqrt(jnp.mean(wide * wide, axis=-1, keepdims=True) + EPS)
    rows_ref[...] = (wide * scale * fgain_ref[...]).astype(BF16)

    seven = held.at[0, 0, pl.ds(0, NZ - 1)]
    pltpu.make_async_copy(seven, seven, own_send).wait()
    three = held.at[0, pl.ds(0, NY - 1)]
    pltpu.make_async_copy(three, three, fwd_send).wait()
    for g in range(NY):
        group = held.at[c, g]
        pltpu.make_async_copy(group, group, pair_send.at[g]).wait()


def attention(qn, qr, lat, keys, cosine, sine, gain, upk, upv, res, fgain, ow):
    vmem = pl.BlockSpec(memory_space=pltpu.VMEM)
    return pl.pallas_call(
        attention_kernel,
        out_shape=[jax.ShapeDtypeStruct(res.shape, BF16)] * 2,
        in_specs=[vmem] * 11 + [pl.BlockSpec(memory_space=pl.ANY)],
        out_specs=[vmem] * 2,
        scratch_shapes=[
            pltpu.VMEM((2, NY, NZ, 128, 128), BF16),
            pltpu.VMEM((QROWS, 256), BF16),
            pltpu.VMEM((GROUP, 256), BF16),
            pltpu.VMEM((VROWS, GROUP), BF16),
            pltpu.VMEM((QROWS // CHUNK, GROUP, CHUNK), F32),
            pltpu.VMEM((QROWS // CHUNK, GROUP, CHUNK), BF16),
            pltpu.VMEM((VROWS, QROWS), F32),
            pltpu.VMEM((1, QROWS), F32),
            pltpu.VMEM(ow.shape, BF16),
            pltpu.SemaphoreType.DMA,
            pltpu.SemaphoreType.DMA,
            pltpu.SemaphoreType.DMA((NY,)),
            pltpu.SemaphoreType.DMA((NZ,)),
            pltpu.SemaphoreType.DMA((NY,)),
            pltpu.SemaphoreType.DMA((NY,)),
            pltpu.SemaphoreType.DMA,
        ],
        compiler_params=pltpu.CompilerParams(
            collective_id=0, has_side_effects=True, vmem_limit_bytes=56 * 2**20
        ),
    )(qn, qr, lat, keys, cosine, sine, gain, upk, upv, res, fgain, ow)


def local(
    residual,
    query_nope,
    query_rope,
    latent,
    rope_key,
    latent_gain,
    up_key,
    up_value,
    out_weight,
    ffn_gain,
    routes,
    route_weight,
    gate_weight,
    up_weight,
    down_weight,
):
    tokens = residual.shape[1]
    width = residual.shape[2]
    experts = lax.axis_size(SP)
    slots = min(tokens, max(2, 5 * tokens * TOPK // (4 * experts)))
    row, lane = iota((128, 128), 0), iota((128, 128), 1)
    token = jnp.where(row < TOK, row, row - TOK + 32 * (lane // ROPE))
    position = (lax.axis_index(SP) * tokens + token).astype(F32)
    freq = (lane % (ROPE // 2)).astype(F32)
    angle = position * ROPE_BASE ** (-freq * 2.0 / ROPE)
    cosine = jnp.cos(angle)
    sine = jnp.where(lane % ROPE < ROPE // 2, -1.0, 1.0) * jnp.sin(angle)
    keys = jnp.transpose(rope_key[0].reshape(TOK // 32, 32, ROPE), (1, 0, 2)).reshape(32, TOK)
    keys = jnp.pad(keys, ((0, 0), (0, 128 - TOK)))
    middle, normal_rows = attention(
        query_nope[0], query_rope[0], latent[0], keys, cosine, sine,
        latent_gain[None], up_key, up_value, residual[0], ffn_gain[None], out_weight,
    )
    middle_wide = middle.astype(jnp.float32)
    own_picks = lax.dynamic_index_in_dim(routes, lax.axis_index("tp"), 0, keepdims=False)
    own_target = assign(own_picks, slots, experts)
    outgoing = pack_rows(normal_rows, own_target, slots, experts).reshape(1, experts, slots, width)
    arrived = lax.all_to_all(outgoing, SP, split_axis=1, concat_axis=1, tiled=True)

    def partial_rows(piece, start):
        return expert_term(piece.reshape(-1, width), gate_weight[0], up_weight[0], down_weight[0])

    terms = on_gathered_pieces(arrived, "tp", 0, partial_rows, 0)
    mine = sent_and_summed(terms.astype(jnp.bfloat16), "tp", 0)
    returned = lax.all_to_all(
        mine.astype(jnp.bfloat16).reshape(1, experts, slots, width),
        SP,
        split_axis=1,
        concat_axis=1,
        tiled=True,
    )
    picked = returned.reshape(experts * slots, width)[own_target].reshape(tokens, TOPK, width)
    combined = jnp.sum(picked.astype(jnp.float32) * route_weight[0][:, :, None], axis=1)
    return (middle_wide + combined).astype(jnp.bfloat16)[None]


def solution(mesh):
    split = Mesh(mesh.devices.reshape(8, 4, 2, mesh.shape["tp"]), ("sp_0", "sp_1", "sp_2", "tp"))
    in_specs = (
        P("tp", SP, None),
        P("tp", SP, None),
        P("tp", SP, None),
        P("tp", SP, None),
        P("tp", SP, None),
        P(),
        P(),
        P(),
        P(),
        P(),
        P(None, SP, None),
        P("tp", SP, None),
        P(SP, None, "tp"),
        P(SP, None, "tp"),
        P(SP, "tp", None),
    )
    out_specs = P("tp", SP, None)
    return jax.shard_map(local, mesh=split, in_specs=in_specs, out_specs=out_specs, check_vma=False)
```

time: 453 us -> 243 us (0.54)
  matrix products: 132 us -> 8.06 us
  blocking collectives: 160 us -> 77 us
  Pallas kernels: 0 us -> 38 us
  local copies, waits for them, and re-layouts: 40.6 us -> 18.2 us
  other arithmetic: 25.2 us -> 8.28 us
    dot_general x61 -> x0, matrix products: 124 us -> none  [the longest x12 44.9 us: step(): jnp.einsum('hqk,khd->qhd', weights.astype(jnp.bfloat16), values, preferre...]
    all_gather x5 -> x0, blocking collectives: 84.3 us -> none  [gather_axes(): nearer = lax.all_gather(x, axes[-1], axis=dim, tiled=True)]
    pallas_call x0 -> x1, Pallas kernels: none -> 38 us  [attention(): pl.pallas_call(attention_kernel, out_shape=[jax.ShapeDtypeStruct(res.shap...]
    convert_element_type x25 -> x0, local copies, waits for them, and re-layouts: 14 us -> none  [the longest x12 6.52 us: step(): jnp.dot(blocks[0], up_value, preferred_element_type=jnp.float32)]
    reduce_sum x13 -> x0, other arithmetic: 12.6 us -> none  [the longest x12 11.7 us: step(): total = total * shrink + jnp.sum(weights, axis=-1)]
    while x180 -> x0, local copies, waits for them, and re-layouts: 7.53 us -> none
  transfers between devices with their start and end apart: 3 -> 2, of which waited for: 2 -> 2; matrix products, arithmetic and copies ran while one was open for 2% -> 0% of each run, Pallas kernels for 0% -> 0%
where the time goes in v1:
time: 243 us; the launch traced here: 242 us
  blocking collectives  77 us (32%)
  waiting for transfers between devices  67 us (28%)
  Pallas kernels  38 us (16%)
  local copies, waits for them, and re-layouts  18.2 us (7%)
  between operations  13.7 us (6%)
  starting transfers between devices  11.9 us (5%)
  other arithmetic  8.28 us (3%)
  matrix products  8.06 us (3%)
    all_to_all x1, blocking collectives, sent_and_summed(): pieces = lax.all_to_all(split_up(x, dim, size), axis, 0, 0, tiled=True)  39.9 us
    all_gather x1, waiting for transfers between devices, on_gathered_pieces(): blocks = [lax.all_gather(section, axis) for section in pieces]  38.9 us
    pallas_call x1, Pallas kernels, attention(): pl.pallas_call(attention_kernel, out_shape=[jax.ShapeDtypeStruct(res.shap...  38 us
    all_to_all x1, blocking collectives, local(): lax.all_to_all(outgoing, SP, split_axis=1, concat_axis=1, tiled=True)  37.1 us
    all_to_all x1, waiting for transfers between devices, local(): lax.all_to_all(mine.astype(jnp.bfloat16).reshape(1, experts, slots, width...  28 us
    all_to_all x1, starting transfers between devices, local(): lax.all_to_all(mine.astype(jnp.bfloat16).reshape(1, experts, slots, width...  11.9 us
  transfers between devices with their start and end apart: 2, of which 2 were waited for; matrix products, arithmetic and copies ran while one was open for 0% of the time, Pallas kernels for 0%

profile of v1, /device:TPU:1, one launch (start us, length us, event | category | flops | bytes accessed | tf_op | source)
XLA Modules:
  0.0 242.1 jit_solution(8298731014195984659)
XLA Ops:
  6.6 0.8 broadcast_multiply_fusion
  7.4 0.1 copy.29
  7.5 0.1 eq.25
  7.7 0.6 reduce-window.6
  8.3 0.2 slice_reduce_fusion
  8.7 0.1 mul.70
  8.9 1.2 scatter_custom_fusion
  10.1 0.8 reshape_squeeze.3
  10.9 0.1 copy.27
  11.1 0.6 pad.9.key_ref
  11.7 1.0 sine_multiply_fusion
  12.7 38.0 %shard_map.145 = (bf16[96,2048]{1,0:T(8,128)(2,1)}, bf16[96,2048]{1,0:T(8,128)(2,1)}) custom-call(bf16[96,1024]{1,0:T(8,128)(2,1)} %bitcast.51, bf16[96,512]{1,0:T(8,128)(2,1)} %bitcast.53, bf16[96,128]{1,0:T(8,128)(2,1)} %bitcast.54, bf16[32,128]{1,0:T(8,128)(2,1)} %pad.9.key_ref, f32[128,128]{1,0:T(8,128)} %get-tuple-element.12.cos_ref, ...), custom_call_target="tpu_custom_call" | custom-call | tf_op jit(solution)/shard_map/pallas_call | solution.py:263
  50.7 1.0 concatenate.3
  51.7 1.1 gather_fusion
  52.9 0.5 reshape.70
  53.4 37.1 %all_to_all.15 = bf16[1,64,3,2048]{3,2,0,1:T(4,128)(2,1)S(1)} all-to-all(bf16[1,64,3,2048]{3,2,0,1:T(4,128)(2,1)S(1)} %bitcast.46), channel_id=1, replica_groups=mesh['sp_0'=8,'sp_1'=4,'sp_2'=2,'tp'=4] {'sp_0','sp_1','sp_2'}, dimensions={1} | all-to-all | bytes 1572864 | tf_op jit(solution)/shard_map/all_to_all | solution.py:330
  90.5 1.5 copy.33
  92.0 38.9 %all-gather.3.cloned.1.call-done = bf16[4,64,3,2048]{3,1,2,0:T(8,128)(2,1)} async-done(((bf16[1,64,3,2048]{3,1,2,0:T(8,128)(2,1)}), bf16[4,64,3,2048]{3,1,2,0:T(8,128)(2,1)}) %all-gather.3.cloned.1.call-update) | async-done | bytes 3145744 | tf_op jit(solution)/shard_map/all_gather | solution.py:54
  130.9 4.3 %copy.34 = bf16[4,64,3,2048]{3,0,2,1:T(4,128)(2,1)S(1)} copy(bf16[4,64,3,2048]{3,1,2,0:T(8,128)(2,1)} %all-gather.3.cloned.1.call-done) | data formatting | bytes 6291456 | tf_op jit(solution)/shard_map/all_gather | solution.py:54
  135.2 3.5 %fusion.4 = f32[4,192,256]{2,1,0:T(8,128)S(1)} fusion(bf16[4,192,2048]{2,0,1:T(4,128)(2,1)S(1)} %bitcast.47, bf16[1,2048,256]{2,1,0:T(8,128)(2,1)S(1)} %copy-done.3), kind=kOutput, calls=%fused_computation.9 | convolution fusion | flops 805502976 | bytes 4980736 | tf_op jit(solution)/shard_map/vmap()/dot_general | solution.py:71
  138.8 3.6 %fusion.16 = bf16[4,192,256]{2,1,0:T(8,128)(2,1)S(1)} fusion(bf16[4,192,2048]{2,0,1:T(4,128)(2,1)S(1)} %bitcast.48, bf16[1,2048,256]{2,1,0:T(8,128)(2,1)S(1)} %copy-done.4, f32[4,192,256]{2,1,0:T(8,128)S(1)} %fusion.4), kind=kOutput, calls=%fused_computation.13 | convolution fusion | flops 807075840 | bytes 5373952 | tf_op jit(solution)/shard_map/vmap()/dot_general | solution.py:72
  142.3 1.0 convolution_convert_fusion
  143.3 39.9 %all_to_all.16 = bf16[4,192,2048]{2,1,0:T(8,128)(2,1)} all-to-all(bf16[4,192,2048]{2,1,0:T(8,128)(2,1)S(1)} %bitcast.45), channel_id=1, replica_groups=mesh['sp_0'=8,'sp_1'=4,'sp_2'=2,'tp'=4] {'tp'}, dimensions={0} | all-to-all | bytes 6291456 | tf_op jit(solution)/shard_map/all_to_all | solution.py:66
  183.3 2.6 %reduce_sum.34 = bf16[192,2048]{1,0:T(8,128)(2,1)S(1)} reduce(bf16[4,192,2048]{2,1,0:T(8,128)(2,1)} %all_to_all.16, bf16[]{:T(256)} %constant.101.clone.1), dimensions={0}, to_apply=%region_4.5 | reduce | flops 1179648 | bytes 3932162 | tf_op jit(solution)/shard_map/reduce_sum | solution.py:67
  185.8 1.3 reshape.73
  187.2 11.9 %all-to-all-start.2 = ((bf16[1,64,3,2048]{3,2,0,1:T(4,128)(2,1)}), bf16[1,64,3,2048]{3,2,0,1:T(4,128)(2,1)S(1)}, u32[]{:S(2)}, u32[]{:S(2)}) async-start(bf16[1,64,3,2048]{3,2,0,1:T(4,128)(2,1)} %bitcast.19), calls=%async_computation.2 | async-start | bytes 2097152 | tf_op jit(solution)/shard_map/all_to_all | solution.py:337
  199.2 28.0 %all-to-all-done.2 = bf16[1,64,3,2048]{3,2,0,1:T(4,128)(2,1)S(1)} async-done(((bf16[1,64,3,2048]{3,2,0,1:T(4,128)(2,1)}), bf16[1,64,3,2048]{3,2,0,1:T(4,128)(2,1)S(1)}, u32[]{:S(2)}, u32[]{:S(2)}) %all-to-all-start.2) | async-done | bytes 786464 | tf_op jit(solution)/shard_map/all_to_all | solution.py:337
  227.3 0.7 reshape.74
  227.9 2.0 gather_fusion.1
  230.0 2.2 reshape.76
  232.2 2.3 multiply_reduce_fusion
  234.5 0.8 fusion.22
  (32 shorter events, 0.6 us)
Async XLA Ops:
  6.5 135.8 %copy-start = (bf16[1,256,2048]{2,1,0:T(8,128)(2,1)S(1)}, bf16[1,256,2048]{2,1,0:T(8,128)(2,1)}, u32[]{:S(2)}) copy-start(bf16[1,256,2048]{2,1,0:T(8,128)(2,1)} %param.29) | copy-start | bytes 3145732
  6.5 124.4 %all-gather.3.cloned.1.call-start = ((), (), s32[]{:S(2)}) async-start(), calls=%async_computation.3 | async-start | bytes 3932160 | tf_op jit(solution)/shard_map/all_gather | solution.py:54
  92.0 43.2 %copy-start.3 = (bf16[1,2048,256]{2,1,0:T(8,128)(2,1)S(1)}, bf16[1,2048,256]{2,1,0:T(8,128)(2,1)}, u32[]{:S(2)}) copy-start(bf16[1,2048,256]{2,1,0:T(8,128)(2,1)} %param.27) | copy-start | bytes 3145732
  135.2 3.5 %copy-start.4 = (bf16[1,2048,256]{2,1,0:T(8,128)(2,1)S(1)}, bf16[1,2048,256]{2,1,0:T(8,128)(2,1)}, u32[]{:S(2)}) copy-start(bf16[1,2048,256]{2,1,0:T(8,128)(2,1)} %param.28) | copy-start | bytes 3145732
  183.3 15.8 %copy-start.2 = (f32[1,96,2]{1,2,0:T(2,128)S(1)}, f32[1,96,2]{1,2,0:T(2,128)}, u32[]{:S(2)}) copy-start(f32[1,96,2]{1,2,0:T(2,128)} %param.26) | copy-start | bytes 2308
  187.2 40.1 %all-to-all-start.2 = ((bf16[1,64,3,2048]{3,2,0,1:T(4,128)(2,1)}), bf16[1,64,3,2048]{3,2,0,1:T(4,128)(2,1)S(1)}, u32[]{:S(2)}, u32[]{:S(2)}) async-start(bf16[1,64,3,2048]{3,2,0,1:T(4,128)(2,1)} %bitcast.19), calls=%async_computation.2 | async-start | bytes 2097152 | tf_op jit(solution)/shard_map/all_to_all | solution.py:337
  230.0 4.5 %copy-start.1 = (bf16[96,2048]{1,0:T(8,128)(2,1)S(1)}, bf16[96,2048]{1,0:T(8,128)(2,1)}, u32[]{:S(2)}) copy-start(bf16[96,2048]{1,0:T(8,128)(2,1)} %get-tuple-element.7) | copy-start | bytes 1179652
Sparse Core Ops, SparseCore 0:
  92.1 38.7 all-gather.2

commit v2 on v1

--- a/solution.py
+++ b/solution.py
@@ -32,61 +32,6 @@
 CHUNK = 512
 VROWS = LATENT + 16
 Z_ORDER = (1, 7, 2, 6, 3, 5, 4)
-
-
-def gather_axes(x, axes, dim):
-    if not axes:
-        return x
-    nearer = lax.all_gather(x, axes[-1], axis=dim, tiled=True)
-    return gather_axes(nearer, axes[:-1], dim)
-
-
-def laid_out(pieces, dim):
-    pieces = jnp.moveaxis(pieces, 0, dim)
-    shape = pieces.shape
-    return pieces.reshape(*shape[:dim], shape[dim] * shape[dim + 1], *shape[dim + 2 :])
-
-
-def on_gathered_pieces(x, axis, dim, work, out_dim):
-    width = x.shape[dim]
-    pieces = jnp.split(x, 2, axis=dim) if width % 2 == 0 else [x]
-    initial = jnp.arange(lax.axis_size(axis)) * width
-    blocks = [lax.all_gather(section, axis) for section in pieces]
-    made = [jax.vmap(work)(b, initial + k * (width // len(pieces))) for k, b in enumerate(blocks)]
-    return laid_out(jnp.concatenate(made, axis=out_dim + 1), out_dim)
-
-
-def split_up(x, dim, size):
-    before, after = (x.shape[:dim], x.shape[dim + 1 :])
-    return jnp.moveaxis(x.reshape(*before, size, -1, *after), dim, 0)
-
-
-def sent_and_summed(x, axis, dim):
-    size = lax.axis_size(axis)
-    pieces = lax.all_to_all(split_up(x, dim, size), axis, 0, 0, tiled=True)
-    return jnp.sum(pieces.astype(jnp.float32), axis=0)
-
-
-def expert_term(rows, gate_w, up_w, down_w):
-    gate = jnp.minimum(jnp.dot(rows, gate_w, preferred_element_type=jnp.float32), CLAMP)
-    lift = jnp.clip(jnp.dot(rows, up_w, preferred_element_type=jnp.float32), -CLAMP, CLAMP)
-    active = (gate * jax.nn.sigmoid(ALPHA * gate) * (lift + 1.0)).astype(jnp.bfloat16)
-    return jnp.dot(active, down_w, preferred_element_type=jnp.float32)
-
-
-def assign(picks, slots, count):
-    flat = picks.reshape(-1)
-    hot = (flat[:, None] == jnp.arange(count, dtype=jnp.int32)[None, :]).astype(jnp.int32)
-    ranks = jnp.sum((jnp.cumsum(hot, axis=0) - 1) * hot, axis=1)
-    return flat * slots + ranks
-
-
-def pack_rows(rows, target, slots, count):
-    tokens = rows.shape[0]
-    owner = jnp.arange(target.shape[0], dtype=jnp.int32) // (target.shape[0] // tokens)
-    source = jnp.full((count * slots,), tokens, jnp.int32).at[target].set(owner)
-    padded = jnp.concatenate([rows, jnp.zeros((1, rows.shape[1]), rows.dtype)], axis=0)
-    return padded[source]
 
 
 def nt_dot(a, b):
@@ -289,6 +234,281 @@
     )(qn, qr, lat, keys, cosine, sine, gain, upk, upv, res, fgain, ow)
 
 
+CHUNK_ROWS = 3 * 16
+Z_ROWS = 8 * CHUNK_ROWS
+ALL_ROWS = 64 * CHUNK_ROWS
+WIDTH = 2048
+STAGES = 5
+
+
+def mixed_tiles(x, outer, inner):
+    return jnp.concatenate(
+        [
+            jnp.concatenate(
+                [x[16 * a : 16 * a + 16, 128 * j : 128 * j + 128] for a in range(outer)], axis=1
+            )
+            for j in range(inner)
+        ],
+        axis=0,
+    )
+
+
+def side_by_side(x):
+    return jnp.concatenate([x[256 * a : 256 * a + 256] for a in range(x.shape[0] // 256)], axis=1)
+
+
+def stacked(x):
+    return jnp.concatenate([x[:, 128 * a : 128 * a + 128] for a in range(x.shape[1] // 128)], axis=0)
+
+
+def swap_matrix():
+    row, col = iota((256, 256), 0), iota((256, 256), 1)
+    return jnp.where(col == (row % 16) * 16 + row // 16, 1.0, 0.0).astype(BF16)
+
+
+def to_chunks(rows, swap):
+    mixed = mixed_tiles(rows, rows.shape[0] // 16, 16)
+    return stacked(jnp.dot(swap, mixed, preferred_element_type=F32).astype(BF16))
+
+
+def from_chunks(chunks, swap):
+    mixed = jnp.dot(swap, side_by_side(chunks), preferred_element_type=F32).astype(BF16)
+    return mixed_tiles(mixed, 16, chunks.shape[0] // 256)
+
+
+def experts_kernel(
+    rows_ref, mid_ref, routes_ref, rw_ref, gate_hbm, up_hbm, down_hbm,
+    out_ref,
+    packed, rows_in, made, part, sums, back, home, swap_ref, gate_ref, up_ref, down_ref,
+    w_sem, a_send, b_send, f_send, p_send, q_send, e_send,
+    a_recv, b_recv, f_recv, p_recv, q_recv, e_recv,
+):
+    z, y, c = (lax.axis_index(name) for name in SP)
+    x = lax.axis_index("tp")
+    me = (z * NY + y) * 2 + c
+    after, before, across = (lax.rem(x + d, 4) for d in (1, 3, 2))
+    barrier = pltpu.get_barrier_semaphore()
+    copies = [
+        pltpu.make_async_copy(gate_hbm.at[0], gate_ref, w_sem.at[0]),
+        pltpu.make_async_copy(up_hbm.at[0], up_ref, w_sem.at[1]),
+        pltpu.make_async_copy(down_hbm.at[0], down_ref, w_sem.at[2]),
+    ]
+
+    def peer(step, k):
+        dz = jnp.where(lax.rem(step, 2) == 1, (step + 1) // 2, NZ - step // 2)
+        pz, py, pc = lax.rem(z + dz, NZ), lax.rem(y + k // 2, NY), lax.rem(c + k, 2)
+        return {"sp_0": pz, "sp_1": py, "sp_2": pc}, (pz * NY + py) * 2 + pc
+
+    def group_of(step):
+        dz = jnp.where(lax.rem(step, 2) == 1, (step + 1) // 2, NZ - step // 2)
+        return lax.rem(z + NZ - lax.rem(dz, NZ), NZ)
+
+    def greet(n, _):
+        pl.semaphore_signal(barrier, inc=1, device_id=peer(n // 8, lax.rem(n, 8))[0], device_id_type=MESH)
+        return 0
+
+    lax.fori_loop(1, 64, greet, 0)
+    for other in (after, before):
+        pl.semaphore_signal(barrier, inc=1, device_id={"tp": other}, device_id_type=MESH)
+    for copy in copies:
+        copy.start()
+
+    swap_ref[...] = swap_matrix()
+    swap = swap_ref[...]
+    picks = routes_ref[x].astype(F32)
+    down_i, right_i = iota((TOK, TOK), 0), iota((TOK, TOK), 1)
+    col = [picks[:, k : k + 1] for k in range(TOPK)]
+    row = [
+        jnp.sum(jnp.where(down_i == right_i, col[k], 0.0), axis=0, keepdims=True)
+        for k in range(TOPK)
+    ]
+    earlier_r = jnp.where(down_i < right_i, 1.0, 0.0)
+    earlier_c = jnp.where(right_i < down_i, 1.0, 0.0)
+
+    def same(a, b):
+        return jnp.where(a == b, 1.0, 0.0)
+
+    rank_row = [
+        jnp.sum(same(col[0], row[0]) * earlier_r, axis=0, keepdims=True),
+        jnp.sum(same(col[0], row[1]) + same(col[1], row[1]) * earlier_r, axis=0, keepdims=True),
+    ]
+    rank_col = [
+        jnp.sum(same(row[0], col[0]) * earlier_c, axis=1, keepdims=True),
+        jnp.sum(same(row[0], col[1]) + same(row[1], col[1]) * earlier_c, axis=1, keepdims=True),
+    ]
+    slot_d = iota((2 * TOK, TOK), 0).astype(F32)
+    spread = sum(same(slot_d, 3.0 * row[k] + rank_row[k]) for k in range(TOPK)).astype(BF16)
+    sent = jnp.dot(spread, rows_ref[...], preferred_element_type=F32).astype(BF16)
+    packed[...] = to_chunks(sent, swap)
+
+    pl.semaphore_wait(barrier, 65)
+
+    def block(index):
+        return pl.ds(pl.multiple_of(index * CHUNK_ROWS, CHUNK_ROWS), CHUNK_ROWS)
+
+    def group(g, half=None):
+        if half is None:
+            return pl.ds(pl.multiple_of(g * Z_ROWS, Z_ROWS), Z_ROWS)
+        return pl.ds(pl.multiple_of(g * Z_ROWS + half * (Z_ROWS // 2), Z_ROWS // 2), Z_ROWS // 2)
+
+    own_copy = pltpu.make_async_copy(packed.at[block(me)], rows_in.at[x, block(me)], a_recv.at[z])
+    own_copy.start()
+
+    def dispatch(n, _):
+        where, index = peer(n // 8, lax.rem(n, 8))
+        pltpu.make_async_remote_copy(
+            src_ref=packed.at[block(index)], dst_ref=rows_in.at[x, block(me)],
+            send_sem=a_send, recv_sem=a_recv.at[z], device_id=where, device_id_type=MESH,
+        ).start()
+        return 0
+
+    lax.fori_loop(1, 64, dispatch, 0)
+    for copy in copies:
+        copy.wait()
+
+    def send(src, dst, ssem, rsem, other):
+        pltpu.make_async_remote_copy(
+            src_ref=src, dst_ref=dst, send_sem=ssem, recv_sem=rsem,
+            device_id={"tp": other}, device_id_type=MESH,
+        ).start()
+
+    def await_(ref, sem):
+        pltpu.make_async_copy(ref, ref, sem).wait()
+
+    sides = ((0, after), (1, before))
+
+    def turn(t, _):
+        @pl.when(t < NZ)
+        def _():
+            g = group_of(t)
+            ref = rows_in.at[x, group(g)]
+            await_(ref, a_recv.at[g])
+            for side, other in sides:
+                send(ref, ref, b_send, b_recv.at[side, g], other)
+
+        @pl.when((t >= 1) & (t < NZ + 1))
+        def _():
+            g = group_of(t - 1)
+            for side, other in sides:
+                origin = before if side == 0 else after
+                await_(rows_in.at[origin, group(g)], b_recv.at[side, g])
+                ref = rows_in.at[origin, group(g, side)]
+                send(ref, ref, f_send, f_recv.at[side, g], other)
+
+        @pl.when((t >= 2) & (t < NZ + 2))
+        def _():
+            g = group_of(t - 2)
+            for side, _other in sides:
+                await_(rows_in.at[across, group(g, side)], f_recv.at[side, g])
+            chunks = jnp.concatenate([rows_in[s, group(g)] for s in range(4)], axis=0)
+            rows = from_chunks(chunks, swap_ref[...])
+            gate = jnp.minimum(jnp.dot(rows, gate_ref[...], preferred_element_type=F32), CLAMP)
+            lift = jnp.clip(jnp.dot(rows, up_ref[...], preferred_element_type=F32), -CLAMP, CLAMP)
+            active = (gate * jax.nn.sigmoid(ALPHA * gate) * (lift + 1.0)).astype(BF16)
+            result = jnp.dot(active, down_ref[...], preferred_element_type=F32).astype(BF16)
+            chunks = to_chunks(result, swap_ref[...])
+            for s in range(4):
+                made[s, group(g)] = chunks[Z_ROWS * s : Z_ROWS * s + Z_ROWS]
+            for side, other in sides:
+                send(made.at[across, group(g, side)], part.at[side, g], p_send, p_recv.at[side, g], other)
+
+        @pl.when((t >= 3) & (t < NZ + 3))
+        def _():
+            g = group_of(t - 3)
+            for side, other in sides:
+                await_(part.at[side, g], p_recv.at[side, g])
+                add = made[other, group(g, side)].astype(F32) + part[side, g].astype(F32)
+                made[other, group(g, side)] = add.astype(BF16)
+                send(made.at[other, group(g)], sums.at[side, g], q_send, q_recv.at[side, g], other)
+
+        @pl.when(t >= 4)
+        def _():
+            g = group_of(t - 4)
+            for side, _other in sides:
+                await_(sums.at[side, g], q_recv.at[side, g])
+            total = made[x, group(g)].astype(F32) + sums[0, g].astype(F32) + sums[1, g].astype(F32)
+            back[group(g)] = total.astype(BF16)
+
+            def give(k, _):
+                py, pc = lax.rem(y + k // 2, NY), lax.rem(c + k, 2)
+                index = (g * NY + py) * 2 + pc
+                is_me = index == me
+
+                @pl.when(is_me)
+                def _():
+                    pltpu.make_async_copy(
+                        back.at[block(me)], home.at[block(me)], e_recv.at[z]
+                    ).start()
+
+                @pl.when(jnp.logical_not(is_me))
+                def _():
+                    pltpu.make_async_remote_copy(
+                        src_ref=back.at[block(index)], dst_ref=home.at[block(me)],
+                        send_sem=e_send, recv_sem=e_recv.at[z],
+                        device_id={"sp_0": g, "sp_1": py, "sp_2": pc}, device_id_type=MESH,
+                    ).start()
+
+                return 0
+
+            lax.fori_loop(0, 8, give, 0)
+
+        return 0
+
+    lax.fori_loop(0, NZ + STAGES - 1, turn, 0)
+
+    slot_c = iota((TOK, 2 * TOK), 1).astype(F32)
+    weight = sum(
+        same(slot_c, 3.0 * col[k] + rank_col[k]) * rw_ref[:, k : k + 1] for k in range(TOPK)
+    )
+    high = weight.astype(BF16)
+    low = (weight - high.astype(F32)).astype(BF16)
+    for g in range(NZ):
+        await_(home.at[group(g)], e_recv.at[g])
+    results = from_chunks(home[...], swap_ref[...])
+    combined = jnp.dot(high, results, preferred_element_type=F32) + jnp.dot(
+        low, results, preferred_element_type=F32
+    )
+    out_ref[...] = (mid_ref[...].astype(F32) + combined).astype(BF16)
+
+    most = pl.ds(0, ALL_ROWS - CHUNK_ROWS)
+    await_(packed.at[most], a_send)
+    await_(back.at[most], e_send)
+    await_(rows_in.at[pl.ds(0, 2)], b_send)
+    await_(rows_in.at[0], f_send)
+    await_(made.at[0], p_send)
+    await_(made.at[pl.ds(0, 2)], q_send)
+
+
+def run_experts(rows, middle, routes, route_weight, gate_weight, up_weight, down_weight):
+    vmem = pl.BlockSpec(memory_space=pltpu.VMEM)
+    anywhere = pl.BlockSpec(memory_space=pl.ANY)
+    dma = pltpu.SemaphoreType.DMA
+    return pl.pallas_call(
+        experts_kernel,
+        out_shape=jax.ShapeDtypeStruct(middle.shape, BF16),
+        in_specs=[vmem] * 4 + [anywhere] * 3,
+        out_specs=vmem,
+        scratch_shapes=[
+            pltpu.VMEM((ALL_ROWS, 128), BF16),
+            pltpu.VMEM((4, ALL_ROWS, 128), BF16),
+            pltpu.VMEM((4, ALL_ROWS, 128), BF16),
+            pltpu.VMEM((2, NZ, Z_ROWS // 2, 128), BF16),
+            pltpu.VMEM((2, NZ, Z_ROWS, 128), BF16),
+            pltpu.VMEM((ALL_ROWS, 128), BF16),
+            pltpu.VMEM((ALL_ROWS, 128), BF16),
+            pltpu.VMEM((256, 256), BF16),
+            pltpu.VMEM(gate_weight.shape[1:], BF16),
+            pltpu.VMEM(up_weight.shape[1:], BF16),
+            pltpu.VMEM(down_weight.shape[1:], BF16),
+            dma((3,)), dma, dma, dma, dma, dma, dma,
+            dma((NZ,)), dma((2, NZ)), dma((2, NZ)), dma((2, NZ)), dma((2, NZ)), dma((NZ,)),
+        ],
+        compiler_params=pltpu.CompilerParams(
+            collective_id=1, has_side_effects=True, vmem_limit_bytes=56 * 2**20
+        ),
+    )(rows, middle, routes, route_weight, gate_weight, up_weight, down_weight)
+
+
 def local(
     residual,
     query_nope,
@@ -307,9 +527,6 @@
     down_weight,
 ):
     tokens = residual.shape[1]
-    width = residual.shape[2]
-    experts = lax.axis_size(SP)
-    slots = min(tokens, max(2, 5 * tokens * TOPK // (4 * experts)))
     row, lane = iota((128, 128), 0), iota((128, 128), 1)
     token = jnp.where(row < TOK, row, row - TOK + 32 * (lane // ROPE))
     position = (lax.axis_index(SP) * tokens + token).astype(F32)
@@ -323,27 +540,10 @@
         query_nope[0], query_rope[0], latent[0], keys, cosine, sine,
         latent_gain[None], up_key, up_value, residual[0], ffn_gain[None], out_weight,
     )
-    middle_wide = middle.astype(jnp.float32)
-    own_picks = lax.dynamic_index_in_dim(routes, lax.axis_index("tp"), 0, keepdims=False)
-    own_target = assign(own_picks, slots, experts)
-    outgoing = pack_rows(normal_rows, own_target, slots, experts).reshape(1, experts, slots, width)
-    arrived = lax.all_to_all(outgoing, SP, split_axis=1, concat_axis=1, tiled=True)
-
-    def partial_rows(piece, start):
-        return expert_term(piece.reshape(-1, width), gate_weight[0], up_weight[0], down_weight[0])
-
-    terms = on_gathered_pieces(arrived, "tp", 0, partial_rows, 0)
-    mine = sent_and_summed(terms.astype(jnp.bfloat16), "tp", 0)
-    returned = lax.all_to_all(
-        mine.astype(jnp.bfloat16).reshape(1, experts, slots, width),
-        SP,
-        split_axis=1,
-        concat_axis=1,
-        tiled=True,
+    updated = run_experts(
+        normal_rows, middle, routes, route_weight[0], gate_weight, up_weight, down_weight
     )
-    picked = returned.reshape(experts * slots, width)[own_target].reshape(tokens, TOPK, width)
-    combined = jnp.sum(picked.astype(jnp.float32) * route_weight[0][:, :, None], axis=1)
-    return (middle_wide + combined).astype(jnp.bfloat16)[None]
+    return updated[None]
 
 
 def solution(mesh):

time: 243 us -> 130 us (0.53)
  Pallas kernels: 38 us -> 122 us
  blocking collectives: 77 us -> 0 us
  waiting for transfers between devices: 67 us -> 0 us
  between operations: 13.7 us -> 0.05 us
  local copies, waits for them, and re-layouts: 18.2 us -> 6.23 us
  starting transfers between devices: 11.9 us -> 0 us
  matrix products: 8.06 us -> 0 us
  other arithmetic: 8.28 us -> 1.02 us
    pallas_call x0 -> x1, Pallas kernels: none -> 84.3 us  [run_experts(): pl.pallas_call(experts_kernel, out_shape=jax.ShapeDtypeStruct(middle.shap...]
    all_to_all x2 -> x0, blocking collectives: 77 us -> none  [the longest x1 39.9 us: sent_and_summed(): pieces = lax.all_to_all(split_up(x, dim, size), axis, 0, 0, tiled=True)]
    all_gather x1 -> x0, waiting for transfers between devices: 38.9 us -> none  [on_gathered_pieces(): blocks = [lax.all_gather(section, axis) for section in pieces]]
    all_to_all x1 -> x0, waiting for transfers between devices: 28 us -> none  [local(): lax.all_to_all(mine.astype(jnp.bfloat16).reshape(1, experts, slots, width...]
    all_to_all x1 -> x0, starting transfers between devices: 11.9 us -> none  [local(): lax.all_to_all(mine.astype(jnp.bfloat16).reshape(1, experts, slots, width...]
    dot_general x3 -> x0, matrix products: 8.06 us -> none  [the longest x1 3.57 us: expert_term(): jnp.dot(rows, up_w, preferred_element_type=jnp.float32)]
    reduce_sum x3 -> x0, other arithmetic: 4.88 us -> none  [the longest x1 2.56 us: sent_and_summed(): return jnp.sum(pieces.astype(jnp.float32), axis=0)]
    unnamed x10 -> x3, local copies, waits for them, and re-layouts: 0.02 us -> 4.65 us
  transfers between devices with their start and end apart: 2 -> 0, of which waited for: 2 -> 0; matrix products, arithmetic and copies ran while one was open for 0% -> 0% of each run, Pallas kernels for 0% -> 0%
where the time goes in v2:
time: 130 us
  Pallas kernels  122 us (94%)
  local copies, waits for them, and re-layouts  6.23 us (5%)
    pallas_call x1, Pallas kernels, run_experts(): pl.pallas_call(experts_kernel, out_shape=jax.ShapeDtypeStruct(middle.shap...  84.3 us
    pallas_call x1, Pallas kernels, attention(): pl.pallas_call(attention_kernel, out_shape=[jax.ShapeDtypeStruct(res.shap...  38 us
    unnamed x3, local copies, waits for them, and re-layouts  4.65 us

profile of v2, /device:TPU:1, one launch (start us, length us, event | category | flops | bytes accessed | tf_op | source)
XLA Modules:
  0.0 129.6 jit_solution(2289993640949728293)
XLA Ops:
  0.1 0.8 reshape_squeeze.3
  0.8 0.1 copy.19
  0.9 0.1 reshape.3
  1.0 0.6 pad.4.key_ref
  1.6 1.4 %copy.20 = f32[1,96,2]{2,1,0:T(8,128)} copy(f32[1,96,2]{1,2,0:T(2,128)} %param.26) | data formatting | bytes 1536 | tf_op args[11]
  3.0 1.0 sine_multiply_fusion
  4.0 1.5 %copy.21.routes_ref = s32[4,96,2]{2,1,0:T(8,128)} copy(s32[4,96,2]{1,2,0:T(2,128)} %param.25) | data formatting | bytes 6144 | tf_op args[10]
  5.5 38.0 %shard_map.145 = (bf16[96,2048]{1,0:T(8,128)(2,1)}, bf16[96,2048]{1,0:T(8,128)(2,1)}) custom-call(bf16[96,1024]{1,0:T(8,128)(2,1)} %bitcast.14, bf16[96,512]{1,0:T(8,128)(2,1)} %bitcast.16, bf16[96,128]{1,0:T(8,128)(2,1)} %bitcast.17, bf16[32,128]{1,0:T(8,128)(2,1)} %pad.4.key_ref, f32[128,128]{1,0:T(8,128)} %get-tuple-element.10.cos_ref, ...), custom_call_target="tpu_custom_call" | custom-call | tf_op jit(solution)/shard_map/pallas_call | solution.py:208
  43.5 84.3 %shard_map.146 = bf16[96,2048]{1,0:T(8,128)(2,1)} custom-call(bf16[96,2048]{1,0:T(8,128)(2,1)} %get-tuple-element.7.rows_ref, bf16[96,2048]{1,0:T(8,128)(2,1)} %get-tuple-element.8.mid_ref, s32[4,96,2]{2,1,0:T(8,128)} %copy.21.routes_ref, f32[96,2]{1,0:T(8,128)} %bitcast.13, bf16[1,2048,256]{2,1,0:T(8,128)(2,1)} %gate_hbm.1, bf16[1,2048,256]{2,1,0:T(8,128)(2,1)} %up_hbm.1, ...), custom_call_target="tpu_custom_call" | custom-call | tf_op jit(solution)/shard_map/pallas_call | solution.py:486
  127.9 1.8 %copy.23 = bf16[1,96,2048]{2,1,0:T(8,128)(2,1)} copy(bf16[1,96,2048]{2,1,0:T(8,128)(2,1)} %bitcast.11) | data formatting | bytes 786432
  (6 shorter events, 0.0 us)

commit v3 on v1

v3 whole, which is shorter than its diff:
```python
import math

import jax
import jax.numpy as jnp
import numpy as np
from jax import lax
from jax.experimental import pallas as pl
from jax.experimental.pallas import tpu as pltpu
from jax.sharding import Mesh
from jax.sharding import PartitionSpec as P

HEADS = 16
NOPE = 64
ROPE = 32
VDIM = 64
LATENT = 128
TOPK = 2
SP = ("sp_0", "sp_1", "sp_2")

EPS = 1e-06
ROPE_BASE = 10000.0
CLAMP = 7.0
ALPHA = 1.702
NEG_BIG = -1e30
MESH = pl.DeviceIdType.MESH

F32 = jnp.float32
BF16 = jnp.bfloat16
NZ, NY = 8, 4
TOK = 96
GROUP = NZ * TOK
QROWS = HEADS * TOK
CHUNK = 512
VROWS = LATENT + 16
Z_ORDER = (1, 7, 2, 6, 3, 5, 4)
ROW_ORDER = (0, 1, 2, 6, 5, 4, 3, 7)
FF_BLOCK = 256
ACT_ROWS = 32


def nt_dot(a, b):
    return lax.dot_general(a, b, (((1,), (1,)), ((), ())), preferred_element_type=F32)


def iota(shape, dim):
    return lax.broadcasted_iota(jnp.int32, shape, dim)


def turned(x, cosine, sine):
    low = iota(x.shape, 1) % ROPE < ROPE // 2
    swapped = jnp.where(low, pltpu.roll(x, 128 - ROPE // 2, 1), pltpu.roll(x, ROPE // 2, 1))
    return x * cosine + swapped * sine


CHUNK_ROWS = 3 * 16
Z_ROWS = 8 * CHUNK_ROWS
ALL_ROWS = 64 * CHUNK_ROWS
WIDTH = 2048
STAGES = 4


def mixed_tiles(x, outer, inner):
    return jnp.concatenate(
        [
            jnp.concatenate(
                [x[16 * a : 16 * a + 16, 128 * j : 128 * j + 128] for a in range(outer)], axis=1
            )
            for j in range(inner)
        ],
        axis=0,
    )


def side_by_side(x):
    return jnp.concatenate([x[256 * a : 256 * a + 256] for a in range(x.shape[0] // 256)], axis=1)


def stacked(x):
    return jnp.concatenate([x[:, 128 * a : 128 * a + 128] for a in range(x.shape[1] // 128)], axis=0)


def swap_matrix():
    row, col = iota((256, 256), 0), iota((256, 256), 1)
    return jnp.where(col == (row % 16) * 16 + row // 16, 1.0, 0.0).astype(BF16)


def to_chunks(rows, swap):
    mixed = mixed_tiles(rows, rows.shape[0] // 16, 16)
    return stacked(jnp.dot(swap, mixed, preferred_element_type=F32).astype(BF16))


def from_chunks(chunks, swap):
    mixed = jnp.dot(swap, side_by_side(chunks), preferred_element_type=F32).astype(BF16)
    return mixed_tiles(mixed, 16, chunks.shape[0] // 256)


def layer_kernel(
    gain_ref, fgain_ref, inv_ref, routes_ref, rw_ref,
    res_hbm, qn_hbm, qr_hbm, lat_hbm, key_hbm, upk_hbm, upv_hbm, ow_hbm, gate_hbm, up_hbm, down_hbm,
    out_ref,
    res_ref, qn_ref, qr_ref, lat_ref, key_ref, upk_ref, upv_ref, ow_ref, gate_ref, up_ref, down_ref,
    held, q_ref, k_ref, v_ref, s_ref, p_ref, acc_ref, peak_ref,
    mid_ref, packed, rows_in, act_out, act_in, back, home, swap_ref, mix_ref,
    in_sem, own_send, fwd_send, pair_send, d_send, h_send, a_send, b_send, f_send, g_send, e_send,
    z_recv, y_recv, pair_recv, d_recv, h_recv, a_recv, b_recv, f_recv, g_recv, e_recv,
):
    z, y, c = (lax.axis_index(name) for name in SP)
    x = lax.axis_index("tp")
    me = (z * NY + y) * 2 + c
    after, before, across = (lax.rem(x + d, 4) for d in (1, 3, 2))
    sides = ((0, after, before), (1, before, after))
    barrier = pltpu.get_barrier_semaphore()

    def distance(step):
        dz = 0
        for n, d in enumerate(ROW_ORDER):
            dz = dz + jnp.where(step == n, d, 0)
        return dz

    def peer(step, k):
        pz = lax.rem(z + distance(step), NZ)
        py, pc = lax.rem(y + k // 2, NY), lax.rem(c + k, 2)
        return {"sp_0": pz, "sp_1": py, "sp_2": pc}, (pz * NY + py) * 2 + pc

    def group_of(step):
        return lax.rem(z + NZ - distance(step), NZ)

    def greet(n, _):
        where = peer(n // 8, lax.rem(n, 8))[0]
        pl.semaphore_signal(barrier, inc=1, device_id=where, device_id_type=MESH)
        return 0

    lax.fori_loop(1, 64, greet, 0)
    for other in (after, before, across):
        pl.semaphore_signal(barrier, inc=1, device_id={"tp": other}, device_id_type=MESH)

    loads = {}
    for n, (name, src, dst) in enumerate((
        ("lat", lat_hbm.at[0], lat_ref),
        ("key", key_hbm.at[0], key_ref),
        ("down", down_hbm.at[0], down_ref.at[x]),
        ("qn", qn_hbm.at[0], qn_ref),
        ("qr", qr_hbm.at[0], qr_ref),
        ("upk", upk_hbm, upk_ref),
        ("upv", upv_hbm, upv_ref),
        ("res", res_hbm.at[0], res_ref),
        ("ow", ow_hbm, ow_ref),
        ("gate", gate_hbm.at[0], gate_ref),
        ("up", up_hbm.at[0], up_ref),
    )):
        loads[name] = pltpu.make_async_copy(src, dst, in_sem.at[n])
        loads[name].start()

    def await_(ref, sem):
        pltpu.make_async_copy(ref, ref, sem).wait()

    def send(src, dst, ssem, rsem, where):
        pltpu.make_async_remote_copy(
            src_ref=src, dst_ref=dst, send_sem=ssem, recv_sem=rsem,
            device_id=where, device_id_type=MESH,
        ).start()

    row, lane = iota((128, 128), 0), iota((128, 128), 1)
    token = jnp.where(row < TOK, row, row - TOK + 32 * (lane // ROPE))
    angle = (me * TOK + token).astype(F32) * inv_ref[...]
    cosine = jnp.cos(angle)
    sine = jnp.where(lane % ROPE < ROPE // 2, -1.0, 1.0) * jnp.sin(angle)

    loads["lat"].wait()
    wide = lat_ref[...].astype(F32)
    scale = lax.rsqrt(jnp.mean(wide * wide, axis=-1, keepdims=True) + EPS)
    held[c, y, z, :TOK, :] = (wide * scale * gain_ref[...]).astype(BF16)
    loads["key"].wait()
    raw = key_ref[...]
    keys = jnp.zeros((32, 128), F32)
    for j in range(TOK // 32):
        chosen = jnp.where(iota((32, TOK), 1) == 32 * j + iota((32, TOK), 0), 1.0, 0.0)
        blank = [jnp.zeros((32, TOK), BF16)] * 4
        blank[j] = raw
        keys = keys + nt_dot(chosen.astype(BF16), jnp.concatenate(blank, axis=0))
    held[c, y, z, TOK:, :] = turned(keys, cosine[TOK:], sine[TOK:]).astype(BF16)

    pl.semaphore_wait(barrier, 66)

    def to_y(block):
        for d in (1, 3, 2):
            send(block, block, fwd_send, y_recv.at[y], {"sp_1": lax.rem(y + d, NY)})

    mine = held.at[c, y, z]
    for d in Z_ORDER:
        send(mine, mine, own_send, z_recv.at[z], {"sp_0": lax.rem(z + d, NZ)})
    to_y(mine)

    loads["down"].wait()
    half_ff = FF_BLOCK // 2
    for side, other, _origin in sides:
        for h in (side, 1 - side):
            piece = down_ref.at[x, pl.ds(half_ff * h, half_ff)]
            send(piece, piece, d_send, d_recv.at[side, h], {"tp": other})

    fold = (NOPE + ROPE) ** (-0.5) * math.log2(math.e)
    lane = iota((TOK, 128), 1)
    in_lane, out_lane = iota((128, 128), 0), iota((128, 128), 1)
    for name in ("qn", "qr", "upk"):
        loads[name].wait()
    turned_tiles = []
    for t in range(HEADS * ROPE // 128):
        tile = qr_ref[:, 128 * t : 128 * t + 128].astype(F32)
        turned_tiles.append((turned(tile, cosine[:TOK], sine[:TOK]) * fold).astype(BF16))
    pick = [
        jnp.where((out_lane < TOK) & (in_lane == ROPE * m + out_lane % ROPE), 1.0, 0.0).astype(BF16)
        for m in range(4)
    ]
    for h in range(HEADS):
        t = h // 2
        plain = qn_ref[:, 128 * t : 128 * t + 128]
        half = lane < NOPE if h % 2 == 0 else lane >= NOPE
        plain = jnp.where(half, plain, jnp.zeros_like(plain))
        lifted = nt_dot(plain, upk_ref[:, 128 * t : 128 * t + 128]) * fold
        q_ref[TOK * h : TOK * h + TOK, :128] = lifted.astype(BF16)
        rotary = jnp.dot(turned_tiles[h // 4], pick[h % 4], preferred_element_type=F32)
        q_ref[TOK * h : TOK * h + TOK, 128:] = rotary.astype(BF16)

    acc_ref[...] = jnp.zeros_like(acc_ref)
    peak_ref[...] = jnp.full_like(peak_ref, NEG_BIG)
    v_ref[LATENT:, :] = jnp.ones((VROWS - LATENT, GROUP), BF16)
    swap_ref[...] = swap_matrix()

    for d in Z_ORDER:
        source = lax.rem(z + d, NZ)
        block = held.at[c, y, source]
        await_(block, z_recv.at[source])
        to_y(block)

    def step(s, _):
        k = lax.rem(s + 1, 3)
        dy = jnp.where(s < 2, 0, jnp.where(k == 0, 1, jnp.where(k == 1, 3, 2)))
        gy = lax.rem(y + dy, NY)
        own = (s == 0) | ((s >= 2) & (s <= 4))
        gc = jnp.where(own, c, 1 - c)
        group = held.at[gc, gy]

        @pl.when(own)
        def _():
            @pl.when(s > 0)
            def _():
                await_(group, y_recv.at[gy])

            send(group, group, pair_send.at[gy], pair_recv.at[gy], {"sp_2": 1 - c})

        @pl.when(jnp.logical_not(own))
        def _():
            await_(group, pair_recv.at[gy])

        @pl.when(s == 3)
        def _():
            for side, other, origin in sides:
                piece = down_ref.at[origin, pl.ds(half_ff * side, half_ff)]
                await_(piece, d_recv.at[side, side])
                send(piece, piece, h_send, h_recv.at[side], {"tp": other})

        lane32 = iota((32, 128), 1) // ROPE
        for b in range(NZ):
            k_ref[TOK * b : TOK * b + TOK, :128] = held[gc, gy, b, :TOK, :]
            packed_keys = held[gc, gy, b, TOK:, :]
            for j in range(TOK // 32):
                first = TOK * b + 32 * j
                k_ref[first : first + 32, 128:] = jnp.where(
                    lane32 == j, packed_keys, jnp.zeros_like(packed_keys)
                )
        for b in range(GROUP // 128):
            v_ref[:LATENT, 128 * b : 128 * b + 128] = k_ref[128 * b : 128 * b + 128, :128].T

        for n in range(QROWS // CHUNK):
            cols = slice(CHUNK * n, CHUNK * n + CHUNK)
            s_ref[n] = nt_dot(k_ref[...], q_ref[cols, :])
            old = peak_ref[:, cols]
            top = jnp.maximum(old, jnp.max(s_ref[n], axis=0, keepdims=True))
            shrink = jnp.exp2(old - top)
            peak_ref[:, cols] = top
            p_ref[n] = jnp.exp2(s_ref[n] - top).astype(BF16)
            mixed = jnp.dot(v_ref[...], p_ref[n], preferred_element_type=F32)
            acc_ref[:, cols] = acc_ref[:, cols] * shrink + mixed
        return 0

    lax.fori_loop(0, 2 * NY, step, 0)

    lat_t = acc_ref[:LATENT, :] / acc_ref[LATENT : LATENT + 1, :]
    mixed_rows = jnp.concatenate(
        [lat_t[:, 128 * b : 128 * b + 128].T for b in range(QROWS // 128)], axis=0
    ).astype(BF16)
    tiles = []
    loads["upv"].wait()
    for t in range(HEADS // 2):
        up = upv_ref[:, 128 * t : 128 * t + 128]
        even = jnp.dot(mixed_rows[192 * t : 192 * t + 96], up, preferred_element_type=F32)
        odd = jnp.dot(mixed_rows[192 * t + 96 : 192 * t + 192], up, preferred_element_type=F32)
        tiles.append(jnp.where(lane < VDIM, even, odd).astype(BF16))
    attended = jnp.concatenate(tiles, axis=1)
    loads["ow"].wait()
    loads["res"].wait()
    projected = jnp.dot(attended, ow_ref[...], preferred_element_type=F32)
    middle = (res_ref[...].astype(F32) + projected).astype(BF16)
    mid_ref[...] = middle
    wide = middle.astype(F32)
    scale = lax.rsqrt(jnp.mean(wide * wide, axis=-1, keepdims=True) + EPS)
    normal_rows = (wide * scale * fgain_ref[...]).astype(BF16)

    picks = routes_ref[x].astype(F32)
    down_i, right_i = iota((TOK, TOK), 0), iota((TOK, TOK), 1)

    def as_column(line):
        return jnp.sum(jnp.where(down_i == right_i, line, 0.0), axis=1, keepdims=True)

    row = [picks[k : k + 1, :] for k in range(TOPK)]
    col = [as_column(line) for line in row]
    earlier_r = jnp.where(down_i < right_i, 1.0, 0.0)
    earlier_c = jnp.where(right_i < down_i, 1.0, 0.0)

    def same(a, b):
        return jnp.where(a == b, 1.0, 0.0)

    rank_row = [
        jnp.sum(same(col[0], row[0]) * earlier_r, axis=0, keepdims=True),
        jnp.sum(same(col[0], row[1]) + same(col[1], row[1]) * earlier_r, axis=0, keepdims=True),
    ]
    rank_col = [
        jnp.sum(same(row[0], col[0]) * earlier_c, axis=1, keepdims=True),
        jnp.sum(same(row[0], col[1]) + same(row[1], col[1]) * earlier_c, axis=1, keepdims=True),
    ]
    slot_d = iota((2 * TOK, TOK), 0).astype(F32)
    spread = sum(same(slot_d, 3.0 * row[k] + rank_row[k]) for k in range(TOPK)).astype(BF16)
    sent = jnp.dot(spread, normal_rows, preferred_element_type=F32).astype(BF16)
    packed[...] = to_chunks(sent, swap_ref[...])
    slot_c = iota((TOK, 2 * TOK), 1).astype(F32)
    weight = sum(
        same(slot_c, 3.0 * col[k] + rank_col[k]) * as_column(rw_ref[k : k + 1, :])
        for k in range(TOPK)
    )
    high = weight.astype(BF16)
    mix_ref[0] = high
    mix_ref[1] = (weight - high.astype(F32)).astype(BF16)

    def block(index):
        return pl.ds(pl.multiple_of(index * CHUNK_ROWS, CHUNK_ROWS), CHUNK_ROWS)

    def group(g, half=None):
        if half is None:
            return pl.ds(pl.multiple_of(g * Z_ROWS, Z_ROWS), Z_ROWS)
        return pl.ds(pl.multiple_of(g * Z_ROWS + half * (Z_ROWS // 2), Z_ROWS // 2), Z_ROWS // 2)

    pltpu.make_async_copy(packed.at[block(me)], rows_in.at[x, block(me)], a_recv.at[z]).start()

    def dispatch(n, _):
        where, index = peer(n // 8, lax.rem(n, 8))
        send(packed.at[block(index)], rows_in.at[x, block(me)], a_send, a_recv.at[z], where)
        return 0

    lax.fori_loop(1, 64, dispatch, 0)

    await_(held.at[0, 0, pl.ds(0, NZ - 1)], own_send)
    await_(held.at[0, pl.ds(0, NY - 1)], fwd_send)
    for g in range(NY):
        await_(held.at[c, g], pair_send.at[g])
    for name in ("gate", "up"):
        loads[name].wait()
    for side, _other, origin in sides:
        await_(down_ref.at[origin, pl.ds(half_ff * (1 - side), half_ff)], d_recv.at[side, 1 - side])
        await_(down_ref.at[across, pl.ds(half_ff * side, half_ff)], h_recv.at[side])
    await_(down_ref.at[pl.ds(0, 2)], d_send)
    await_(down_ref.at[0], h_send)

    def turn(t, _):
        @pl.when(t < NZ)
        def _():
            g = group_of(t)
            ref = rows_in.at[x, group(g)]
            await_(ref, a_recv.at[g])
            for side, other, _origin in sides:
                send(ref, ref, b_send, b_recv.at[side, g], {"tp": other})

        @pl.when((t >= 1) & (t < NZ + 1))
        def _():
            g = group_of(t - 1)
            for side, other, origin in sides:
                await_(rows_in.at[origin, group(g)], b_recv.at[side, g])
                ref = rows_in.at[origin, group(g, side)]
                send(ref, ref, f_send, f_recv.at[side, g], {"tp": other})

        @pl.when((t >= 2) & (t < NZ + 2))
        def _():
            g = group_of(t - 2)
            for side, _other, _origin in sides:
                await_(rows_in.at[across, group(g, side)], f_recv.at[side, g])
            chunks = jnp.concatenate([rows_in[s, group(g)] for s in range(4)], axis=0)
            rows = from_chunks(chunks, swap_ref[...])
            gate = jnp.minimum(jnp.dot(rows, gate_ref[...], preferred_element_type=F32), CLAMP)
            lift = jnp.clip(jnp.dot(rows, up_ref[...], preferred_element_type=F32), -CLAMP, CLAMP)
            active = gate * jax.nn.sigmoid(ALPHA * gate) * (lift + 1.0)
            filler = jnp.zeros((ACT_ROWS - 24, FF_BLOCK), F32)
            for s in range(4):
                own_rows = jnp.concatenate([active[24 * s : 24 * s + 24], filler], axis=0)
                act_out[g, s] = own_rows.astype(BF16)
            act_in[g, x] = act_out[g, x]
            for n, other in enumerate((after, before, across)):
                send(act_out.at[g, other], act_in.at[g, x], g_send, g_recv.at[n, g], {"tp": other})

        @pl.when(t >= 3)
        def _():
            g = group_of(t - 3)
            for n, origin in enumerate((before, after, across)):
                await_(act_in.at[g, origin], g_recv.at[n, g])
            acts = jnp.concatenate([act_in[g, s] for s in range(4)], axis=1)
            down = down_ref[...].reshape(4 * FF_BLOCK, WIDTH)
            result = jnp.dot(acts, down, preferred_element_type=F32).astype(BF16)
            back[group(g)] = to_chunks(result, swap_ref[...])[:Z_ROWS]

            def give(k, _):
                py, pc = lax.rem(y + k // 2, NY), lax.rem(c + k, 2)
                index = (g * NY + py) * 2 + pc

                @pl.when(index == me)
                def _():
                    pltpu.make_async_copy(back.at[block(me)], home.at[block(me)], e_recv.at[z]).start()

                @pl.when(index != me)
                def _():
                    where = {"sp_0": g, "sp_1": py, "sp_2": pc}
                    send(back.at[block(index)], home.at[block(me)], e_send, e_recv.at[z], where)

                return 0

            lax.fori_loop(0, 8, give, 0)

        return 0

    lax.fori_loop(0, NZ + STAGES - 1, turn, 0)

    for g in range(NZ):
        await_(home.at[group(g)], e_recv.at[g])
    results = from_chunks(home[...], swap_ref[...])
    combined = jnp.dot(mix_ref[0], results, preferred_element_type=F32) + jnp.dot(
        mix_ref[1], results, preferred_element_type=F32
    )
    out_ref[...] = (mid_ref[...].astype(F32) + combined).astype(BF16)

    most = pl.ds(0, ALL_ROWS - CHUNK_ROWS)
    await_(packed.at[most], a_send)
    await_(back.at[most], e_send)
    await_(rows_in.at[pl.ds(0, 2)], b_send)
    await_(rows_in.at[0], f_send)
    await_(act_in.at[pl.ds(0, 6)], g_send)


def layer(small, large):
    vmem = pl.BlockSpec(memory_space=pltpu.VMEM)
    anywhere = pl.BlockSpec(memory_space=pl.ANY)
    dma = pltpu.SemaphoreType.DMA
    res, qn, qr, lat, key, upk, upv, ow, gate, up, down = large
    held_in = [
        pltpu.VMEM(a.shape[-2:], BF16) for a in (res, qn, qr, lat, key, upk, upv, ow, gate, up)
    ]
    return pl.pallas_call(
        layer_kernel,
        out_shape=jax.ShapeDtypeStruct(res.shape[1:], BF16),
        in_specs=[vmem] * len(small) + [anywhere] * len(large),
        out_specs=vmem,
        scratch_shapes=held_in
        + [
            pltpu.VMEM((4,) + down.shape[1:], BF16),
            pltpu.VMEM((2, NY, NZ, 128, 128), BF16),
            pltpu.VMEM((QROWS, 256), BF16),
            pltpu.VMEM((GROUP, 256), BF16),
            pltpu.VMEM((VROWS, GROUP), BF16),
            pltpu.VMEM((QROWS // CHUNK, GROUP, CHUNK), F32),
            pltpu.VMEM((QROWS // CHUNK, GROUP, CHUNK), BF16),
            pltpu.VMEM((VROWS, QROWS), F32),
            pltpu.VMEM((1, QROWS), F32),
            pltpu.VMEM((TOK, WIDTH), BF16),
            pltpu.VMEM((ALL_ROWS, 128), BF16),
            pltpu.VMEM((4, ALL_ROWS, 128), BF16),
            pltpu.VMEM((NZ, 4, ACT_ROWS, FF_BLOCK), BF16),
            pltpu.VMEM((NZ, 4, ACT_ROWS, FF_BLOCK), BF16),
            pltpu.VMEM((ALL_ROWS, 128), BF16),
            pltpu.VMEM((ALL_ROWS, 128), BF16),
            pltpu.VMEM((256, 256), BF16),
            pltpu.VMEM((2, TOK, 2 * TOK), BF16),
            dma((len(large),)), dma, dma, dma((NY,)), dma, dma, dma, dma, dma, dma, dma,
            dma((NZ,)), dma((NY,)), dma((NY,)), dma((2, 2)), dma((2,)),
            dma((NZ,)), dma((2, NZ)), dma((2, NZ)), dma((3, NZ)), dma((NZ,)),
        ],
        compiler_params=pltpu.CompilerParams(
            collective_id=0, has_side_effects=True, vmem_limit_bytes=60 * 2**20
        ),
    )(*small, *large)


def local(
    residual,
    query_nope,
    query_rope,
    latent,
    rope_key,
    latent_gain,
    up_key,
    up_value,
    out_weight,
    ffn_gain,
    routes,
    route_weight,
    gate_weight,
    up_weight,
    down_weight,
):
    half = ROPE // 2
    inverse = (ROPE_BASE ** (-(np.arange(128) % half) * 2.0 / ROPE)).astype(np.float32)
    small = (
        latent_gain[None],
        ffn_gain[None],
        jnp.asarray(inverse)[None],
        jnp.swapaxes(routes, 1, 2),
        jnp.swapaxes(route_weight[0], 0, 1),
    )
    large = (
        residual, query_nope, query_rope, latent, jnp.swapaxes(rope_key, 1, 2),
        up_key, up_value, out_weight, gate_weight, up_weight, down_weight,
    )
    return layer(small, large)[None]


def solution(mesh):
    split = Mesh(mesh.devices.reshape(8, 4, 2, mesh.shape["tp"]), ("sp_0", "sp_1", "sp_2", "tp"))
    in_specs = (
        P("tp", SP, None),
        P("tp", SP, None),
        P("tp", SP, None),
        P("tp", SP, None),
        P("tp", SP, None),
        P(),
        P(),
        P(),
        P(),
        P(),
        P(None, SP, None),
        P("tp", SP, None),
        P(SP, None, "tp"),
        P(SP, None, "tp"),
        P(SP, "tp", None),
    )
    out_specs = P("tp", SP, None)
    return jax.shard_map(local, mesh=split, in_specs=in_specs, out_specs=out_specs, check_vma=False)
```

time: 243 us -> 104 us (0.43)
  blocking collectives: 77 us -> 0 us
  waiting for transfers between devices: 67 us -> 0 us
  Pallas kernels: 38 us -> 103 us
  local copies, waits for them, and re-layouts: 18.2 us -> 1.77 us
  between operations: 13.7 us -> 0.01 us
  starting transfers between devices: 11.9 us -> 0 us
  other arithmetic: 8.28 us -> 0 us
  matrix products: 8.06 us -> 0 us
    all_to_all x2 -> x0, blocking collectives: 77 us -> none  [the longest x1 39.9 us: sent_and_summed(): pieces = lax.all_to_all(split_up(x, dim, size), axis, 0, 0, tiled=True)]
    pallas_call x1, Pallas kernels: 38 us -> 103 us  [layer(): pl.pallas_call(layer_kernel, out_shape=jax.ShapeDtypeStruct(res.shape[1:]...]
    all_gather x1 -> x0, waiting for transfers between devices: 38.9 us -> none  [on_gathered_pieces(): blocks = [lax.all_gather(section, axis) for section in pieces]]
    all_to_all x1 -> x0, waiting for transfers between devices: 28 us -> none  [local(): lax.all_to_all(mine.astype(jnp.bfloat16).reshape(1, experts, slots, width...]
    all_to_all x1 -> x0, starting transfers between devices: 11.9 us -> none  [local(): lax.all_to_all(mine.astype(jnp.bfloat16).reshape(1, experts, slots, width...]
    dot_general x3 -> x0, matrix products: 8.06 us -> none  [the longest x1 3.57 us: expert_term(): jnp.dot(rows, up_w, preferred_element_type=jnp.float32)]
    reduce_sum x3 -> x0, other arithmetic: 4.88 us -> none  [the longest x1 2.56 us: sent_and_summed(): return jnp.sum(pieces.astype(jnp.float32), axis=0)]
    all_gather x1 -> x0, local copies, waits for them, and re-layouts: 4.32 us -> none  [on_gathered_pieces(): blocks = [lax.all_gather(section, axis) for section in pieces]]
  transfers between devices with their start and end apart: 2 -> 0, of which waited for: 2 -> 0; matrix products, arithmetic and copies ran while one was open for 0% -> 0% of each run, Pallas kernels for 0% -> 0%
where the time goes in v3:
time: 104 us
  Pallas kernels  103 us (99%)
  local copies, waits for them, and re-layouts  1.77 us (2%)
    pallas_call x1, Pallas kernels, layer(): pl.pallas_call(layer_kernel, out_shape=jax.ShapeDtypeStruct(res.shape[1:]...  103 us

profile of v3, /device:TPU:1, one launch (start us, length us, event | category | flops | bytes accessed | tf_op | source)
XLA Modules:
  0.0 104.3 jit_solution(13484815181841529336)
XLA Ops:
  0.0 102.5 %shard_map.154 = bf16[96,2048]{1,0:T(8,128)(2,1)} custom-call(f32[1,128]{1,0:T(1,128)} %bitcast.13, f32[1,2048]{1,0:T(1,128)} %bitcast.9, f32[1,128]{1,0:T(1,128)} %constant.13.inv_ref, s32[4,2,96]{2,1,0:T(2,128)} %bitcast.11, f32[2,96]{1,0:T(2,128)} %bitcast.12, bf16[1,96,2048]{2,1,0:T(8,128)(2,1)} %res_hbm.1, bf16[1,96,1024]{2,1,0:T(8,128)(2,1)} %qn_hbm.1, ...), custom_call_target="tpu_custom_call" | custom-call | tf_op jit(solution)/shard_map/pallas_call | solution.py:463
  102.5 1.8 %copy.18 = bf16[1,96,2048]{2,1,0:T(8,128)(2,1)} copy(bf16[1,96,2048]{2,1,0:T(8,128)(2,1)} %bitcast.8) | data formatting | bytes 786432

commit v4 on v3

--- a/solution.py
+++ b/solution.py
@@ -32,8 +32,9 @@
 QROWS = HEADS * TOK
 CHUNK = 512
 VROWS = LATENT + 16
+KEYS = 256
 Z_ORDER = (1, 7, 2, 6, 3, 5, 4)
-ROW_ORDER = (0, 1, 2, 6, 5, 4, 3, 7)
+ROW_ORDER = (0, 1, 7, 2, 6, 5, 3, 4)
 FF_BLOCK = 256
 ACT_ROWS = 32
 
@@ -95,10 +96,9 @@
 
 
 def layer_kernel(
-    gain_ref, fgain_ref, inv_ref, routes_ref, rw_ref,
-    res_hbm, qn_hbm, qr_hbm, lat_hbm, key_hbm, upk_hbm, upv_hbm, ow_hbm, gate_hbm, up_hbm, down_hbm,
+    gain_hbm, fgain_hbm, inv_hbm, routes_hbm, rw_hbm, res_hbm, qn_hbm, qr_hbm, lat_hbm, key_hbm, upk_hbm, upv_hbm, ow_hbm, gate_hbm, up_hbm, down_hbm,
     out_ref,
-    res_ref, qn_ref, qr_ref, lat_ref, key_ref, upk_ref, upv_ref, ow_ref, gate_ref, up_ref, down_ref,
+    gain_ref, fgain_ref, inv_ref, routes_ref, rw_ref, res_ref, qn_ref, qr_ref, lat_ref, key_ref, upk_ref, upv_ref, ow_ref, gate_ref, up_ref, down_ref,
     held, q_ref, k_ref, v_ref, s_ref, p_ref, acc_ref, peak_ref,
     mid_ref, packed, rows_in, act_out, act_in, back, home, swap_ref, mix_ref,
     in_sem, own_send, fwd_send, pair_send, d_send, h_send, a_send, b_send, f_send, g_send, e_send,
@@ -125,17 +125,16 @@
     def group_of(step):
         return lax.rem(z + NZ - distance(step), NZ)
 
-    def greet(n, _):
-        where = peer(n // 8, lax.rem(n, 8))[0]
+    near = [{"sp_0": lax.rem(z + d, NZ)} for d in Z_ORDER]
+    near += [{"sp_1": lax.rem(y + d, NY)} for d in (1, 3, 2)] + [{"sp_2": 1 - c}]
+    near += [{"tp": other} for other in (after, before, across)]
+    for where in near:
         pl.semaphore_signal(barrier, inc=1, device_id=where, device_id_type=MESH)
-        return 0
-
-    lax.fori_loop(1, 64, greet, 0)
-    for other in (after, before, across):
-        pl.semaphore_signal(barrier, inc=1, device_id={"tp": other}, device_id_type=MESH)
 
     loads = {}
     for n, (name, src, dst) in enumerate((
+        ("inv", inv_hbm, inv_ref),
+        ("gain", gain_hbm, gain_ref),
         ("lat", lat_hbm.at[0], lat_ref),
         ("key", key_hbm.at[0], key_ref),
         ("down", down_hbm.at[0], down_ref.at[x]),
@@ -147,6 +146,9 @@
         ("ow", ow_hbm, ow_ref),
         ("gate", gate_hbm.at[0], gate_ref),
         ("up", up_hbm.at[0], up_ref),
+        ("fgain", fgain_hbm, fgain_ref),
+        ("routes", routes_hbm, routes_ref),
+        ("rw", rw_hbm, rw_ref),
     )):
         loads[name] = pltpu.make_async_copy(src, dst, in_sem.at[n])
         loads[name].start()
@@ -162,6 +164,8 @@
 
     row, lane = iota((128, 128), 0), iota((128, 128), 1)
     token = jnp.where(row < TOK, row, row - TOK + 32 * (lane // ROPE))
+    loads["inv"].wait()
+    loads["gain"].wait()
     angle = (me * TOK + token).astype(F32) * inv_ref[...]
     cosine = jnp.cos(angle)
     sine = jnp.where(lane % ROPE < ROPE // 2, -1.0, 1.0) * jnp.sin(angle)
@@ -180,16 +184,7 @@
         keys = keys + nt_dot(chosen.astype(BF16), jnp.concatenate(blank, axis=0))
     held[c, y, z, TOK:, :] = turned(keys, cosine[TOK:], sine[TOK:]).astype(BF16)
 
-    pl.semaphore_wait(barrier, 66)
-
-    def to_y(block):
-        for d in (1, 3, 2):
-            send(block, block, fwd_send, y_recv.at[y], {"sp_1": lax.rem(y + d, NY)})
-
-    mine = held.at[c, y, z]
-    for d in Z_ORDER:
-        send(mine, mine, own_send, z_recv.at[z], {"sp_0": lax.rem(z + d, NZ)})
-    to_y(mine)
+    pl.semaphore_wait(barrier, len(near))
 
     loads["down"].wait()
     half_ff = FF_BLOCK // 2
@@ -197,6 +192,16 @@
         for h in (side, 1 - side):
             piece = down_ref.at[x, pl.ds(half_ff * h, half_ff)]
             send(piece, piece, d_send, d_recv.at[side, h], {"tp": other})
+
+    def to_y(block, source):
+        for d in (1, 3):
+            where = {"sp_1": lax.rem(y + d, NY)}
+            send(block, block, fwd_send, y_recv.at[y, source // (NZ // 2)], where)
+
+    mine = held.at[c, y, z]
+    for d in Z_ORDER:
+        send(mine, mine, own_send, z_recv.at[z], {"sp_0": lax.rem(z + d, NZ)})
+    to_y(mine, z)
 
     fold = (NOPE + ROPE) ** (-0.5) * math.log2(math.e)
     lane = iota((TOK, 128), 1)
@@ -230,29 +235,43 @@
         source = lax.rem(z + d, NZ)
         block = held.at[c, y, source]
         await_(block, z_recv.at[source])
-        to_y(block)
+        to_y(block, source)
 
     def step(s, _):
-        k = lax.rem(s + 1, 3)
-        dy = jnp.where(s < 2, 0, jnp.where(k == 0, 1, jnp.where(k == 1, 3, 2)))
+        dy = jnp.where(s < 2, 0, jnp.where(s >= 6, 2, jnp.where(lax.rem(s, 2) == 0, 1, 3)))
         gy = lax.rem(y + dy, NY)
-        own = (s == 0) | ((s >= 2) & (s <= 4))
+        own = (s == 0) | (s == 2) | (s == 3) | (s == 6)
         gc = jnp.where(own, c, 1 - c)
         group = held.at[gc, gy]
 
+        def half_column(origin, h):
+            return held.at[c, origin, pl.ds(h * (NZ // 2), NZ // 2)]
+
+        @pl.when(s == 2)
+        def _():
+            for h, d in ((0, 1), (1, 3)):
+                origin = lax.rem(y + NY - d, NY)
+                part = half_column(origin, h)
+                await_(part, y_recv.at[origin, h])
+                send(part, part, fwd_send, y_recv.at[origin, h], {"sp_1": lax.rem(y + d, NY)})
+
+        @pl.when((s == 2) | (s == 6))
+        def _():
+            await_(half_column(gy, 0), y_recv.at[gy, 0])
+
+        @pl.when((s == 3) | (s == 6))
+        def _():
+            await_(half_column(gy, 1), y_recv.at[gy, 1])
+
         @pl.when(own)
         def _():
-            @pl.when(s > 0)
-            def _():
-                await_(group, y_recv.at[gy])
-
             send(group, group, pair_send.at[gy], pair_recv.at[gy], {"sp_2": 1 - c})
 
         @pl.when(jnp.logical_not(own))
         def _():
             await_(group, pair_recv.at[gy])
 
-        @pl.when(s == 3)
+        @pl.when(s == 4)
         def _():
             for side, other, origin in sides:
                 piece = down_ref.at[origin, pl.ds(half_ff * side, half_ff)]
@@ -271,16 +290,42 @@
         for b in range(GROUP // 128):
             v_ref[:LATENT, 128 * b : 128 * b + 128] = k_ref[128 * b : 128 * b + 128, :128].T
 
-        for n in range(QROWS // CHUNK):
-            cols = slice(CHUNK * n, CHUNK * n + CHUNK)
-            s_ref[n] = nt_dot(k_ref[...], q_ref[cols, :])
-            old = peak_ref[:, cols]
-            top = jnp.maximum(old, jnp.max(s_ref[n], axis=0, keepdims=True))
-            shrink = jnp.exp2(old - top)
-            peak_ref[:, cols] = top
-            p_ref[n] = jnp.exp2(s_ref[n] - top).astype(BF16)
+        def cols(n):
+            return slice(CHUNK * n, CHUNK * n + CHUNK)
+
+        def score(n, r):
+            keys = slice(KEYS * r, KEYS * r + KEYS)
+            made = nt_dot(k_ref[keys, :], q_ref[cols(n), :])
+            s_ref[n, keys, :] = made
+            return jnp.max(made.reshape(KEYS // 8, 8, CHUNK), axis=0)
+
+        def raised(n, tops):
+            old = peak_ref[:, cols(n)]
+            most = jnp.maximum(jnp.maximum(tops[0], tops[1]), tops[2])
+            top = jnp.maximum(old, jnp.max(most, axis=0, keepdims=True))
+            peak_ref[:, cols(n)] = top
+            return top, jnp.exp2(old - top)
+
+        def weigh(n, r, top):
+            keys = slice(KEYS * r, KEYS * r + KEYS)
+            p_ref[n, keys, :] = jnp.exp2(s_ref[n, keys, :] - top).astype(BF16)
+
+        def mix(n, shrink):
             mixed = jnp.dot(v_ref[...], p_ref[n], preferred_element_type=F32)
-            acc_ref[:, cols] = acc_ref[:, cols] * shrink + mixed
+            acc_ref[:, cols(n)] = acc_ref[:, cols(n)] * shrink + mixed
+
+        blocks = range(GROUP // KEYS)
+        chunks = QROWS // CHUNK
+        top, shrink = raised(0, [score(0, r) for r in blocks])
+        for n in range(1, chunks + 1):
+            tops = []
+            for r in blocks:
+                if n < chunks:
+                    tops.append(score(n, r))
+                weigh(n - 1, r, top)
+            mix(n - 1, shrink)
+            if n < chunks:
+                top, shrink = raised(n, tops)
         return 0
 
     lax.fori_loop(0, 2 * NY, step, 0)
@@ -297,8 +342,8 @@
         odd = jnp.dot(mixed_rows[192 * t + 96 : 192 * t + 192], up, preferred_element_type=F32)
         tiles.append(jnp.where(lane < VDIM, even, odd).astype(BF16))
     attended = jnp.concatenate(tiles, axis=1)
-    loads["ow"].wait()
-    loads["res"].wait()
+    for name in ("ow", "res", "fgain", "routes", "rw"):
+        loads[name].wait()
     projected = jnp.dot(attended, ow_ref[...], preferred_element_type=F32)
     middle = (res_ref[...].astype(F32) + projected).astype(BF16)
     mid_ref[...] = middle
@@ -347,28 +392,26 @@
     def group(g, half=None):
         if half is None:
             return pl.ds(pl.multiple_of(g * Z_ROWS, Z_ROWS), Z_ROWS)
-        return pl.ds(pl.multiple_of(g * Z_ROWS + half * (Z_ROWS // 2), Z_ROWS // 2), Z_ROWS // 2)
+        first = 3 * CHUNK_ROWS
+        if half == 0:
+            return pl.ds(pl.multiple_of(g * Z_ROWS, CHUNK_ROWS), first)
+        return pl.ds(pl.multiple_of(g * Z_ROWS + first, CHUNK_ROWS), Z_ROWS - first)
 
     pltpu.make_async_copy(packed.at[block(me)], rows_in.at[x, block(me)], a_recv.at[z]).start()
 
     def dispatch(n, _):
         where, index = peer(n // 8, lax.rem(n, 8))
-        send(packed.at[block(index)], rows_in.at[x, block(me)], a_send, a_recv.at[z], where)
+
+        @pl.when(index != me)
+        def _():
+            send(packed.at[block(index)], rows_in.at[x, block(me)], a_send, a_recv.at[z], where)
+
         return 0
 
-    lax.fori_loop(1, 64, dispatch, 0)
-
-    await_(held.at[0, 0, pl.ds(0, NZ - 1)], own_send)
-    await_(held.at[0, pl.ds(0, NY - 1)], fwd_send)
-    for g in range(NY):
-        await_(held.at[c, g], pair_send.at[g])
+    lax.fori_loop(0, 64, dispatch, 0)
+
     for name in ("gate", "up"):
         loads[name].wait()
-    for side, _other, origin in sides:
-        await_(down_ref.at[origin, pl.ds(half_ff * (1 - side), half_ff)], d_recv.at[side, 1 - side])
-        await_(down_ref.at[across, pl.ds(half_ff * side, half_ff)], h_recv.at[side])
-    await_(down_ref.at[pl.ds(0, 2)], d_send)
-    await_(down_ref.at[0], h_send)
 
     def turn(t, _):
         @pl.when(t < NZ)
@@ -408,6 +451,14 @@
         @pl.when(t >= 3)
         def _():
             g = group_of(t - 3)
+
+            @pl.when(t == 3)
+            def _():
+                for side, _other, origin in sides:
+                    rest = pl.ds(half_ff * (1 - side), half_ff)
+                    await_(down_ref.at[origin, rest], d_recv.at[side, 1 - side])
+                    await_(down_ref.at[across, pl.ds(half_ff * side, half_ff)], h_recv.at[side])
+
             for n, origin in enumerate((before, after, across)):
                 await_(act_in.at[g, origin], g_recv.at[n, g])
             acts = jnp.concatenate([act_in[g, s] for s in range(4)], axis=1)
@@ -444,6 +495,12 @@
     )
     out_ref[...] = (mid_ref[...].astype(F32) + combined).astype(BF16)
 
+    await_(held.at[0, 0, pl.ds(0, NZ - 1)], own_send)
+    await_(held.at[0, pl.ds(0, NY - 1)], fwd_send)
+    for g in range(NY):
+        await_(held.at[c, g], pair_send.at[g])
+    await_(down_ref.at[pl.ds(0, 2)], d_send)
+    await_(down_ref.at[0], h_send)
     most = pl.ds(0, ALL_ROWS - CHUNK_ROWS)
     await_(packed.at[most], a_send)
     await_(back.at[most], e_send)
@@ -463,9 +520,10 @@
     return pl.pallas_call(
         layer_kernel,
         out_shape=jax.ShapeDtypeStruct(res.shape[1:], BF16),
-        in_specs=[vmem] * len(small) + [anywhere] * len(large),
+        in_specs=[anywhere] * (len(small) + len(large)),
         out_specs=vmem,
-        scratch_shapes=held_in
+        scratch_shapes=[pltpu.VMEM(a.shape, a.dtype) for a in small]
+        + held_in
         + [
             pltpu.VMEM((4,) + down.shape[1:], BF16),
             pltpu.VMEM((2, NY, NZ, 128, 128), BF16),
@@ -485,8 +543,8 @@
             pltpu.VMEM((ALL_ROWS, 128), BF16),
             pltpu.VMEM((256, 256), BF16),
             pltpu.VMEM((2, TOK, 2 * TOK), BF16),
-            dma((len(large),)), dma, dma, dma((NY,)), dma, dma, dma, dma, dma, dma, dma,
-            dma((NZ,)), dma((NY,)), dma((NY,)), dma((2, 2)), dma((2,)),
+            dma((len(small) + len(large),)), dma, dma, dma((NY,)), dma, dma, dma, dma, dma, dma, dma,
+            dma((NZ,)), dma((NY, 2)), dma((NY,)), dma((2, 2)), dma((2,)),
             dma((NZ,)), dma((2, NZ)), dma((2, NZ)), dma((3, NZ)), dma((NZ,)),
         ],
         compiler_params=pltpu.CompilerParams(

time: 104 us -> 95.4 us (0.917)
  Pallas kernels: 103 us -> 93.5 us
    pallas_call x1, Pallas kernels: 103 us -> 93.5 us  [layer(): pl.pallas_call(layer_kernel, out_shape=jax.ShapeDtypeStruct(res.shape[1:]...]
where the time goes in v4:
time: 95.4 us; the launch traced here: 95.2 us
  Pallas kernels  93.5 us (98%)
  local copies, waits for them, and re-layouts  1.77 us (2%)
    pallas_call x1, Pallas kernels, layer(): pl.pallas_call(layer_kernel, out_shape=jax.ShapeDtypeStruct(res.shape[1:]...  93.5 us

profile of v4, /device:TPU:1, one launch (start us, length us, event | category | flops | bytes accessed | tf_op | source)
XLA Modules:
  0.0 95.2 jit_solution(8902368839009435511)
XLA Ops:
  0.0 93.5 %shard_map.154 = bf16[96,2048]{1,0:T(8,128)(2,1)} custom-call(f32[1,128]{1,0:T(1,128)} %bitcast.13, f32[1,2048]{1,0:T(1,128)} %bitcast.9, f32[1,128]{1,0:T(1,128)} %constant.13.inv_hbm, s32[4,2,96]{2,1,0:T(2,128)} %bitcast.11, f32[2,96]{1,0:T(2,128)} %bitcast.12, bf16[1,96,2048]{2,1,0:T(8,128)(2,1)} %res_hbm.1, bf16[1,96,1024]{2,1,0:T(8,128)(2,1)} %qn_hbm.1, ...), custom_call_target="tpu_custom_call" | custom-call | tf_op jit(solution)/shard_map/pallas_call | solution.py:520
  93.5 1.8 %copy.18 = bf16[1,96,2048]{2,1,0:T(8,128)(2,1)} copy(bf16[1,96,2048]{2,1,0:T(8,128)(2,1)} %bitcast.8) | data formatting | bytes 786432

commit v5 on v4

--- a/solution.py
+++ b/solution.py
@@ -34,9 +34,9 @@
 VROWS = LATENT + 16
 KEYS = 256
 Z_ORDER = (1, 7, 2, 6, 3, 5, 4)
-ROW_ORDER = (0, 1, 7, 2, 6, 5, 3, 4)
+ROW_ORDER = (0, 7, 6, 2, 5, 3, 4, 1)
 FF_BLOCK = 256
-ACT_ROWS = 32
+OWN_ROWS = 24
 
 
 def nt_dot(a, b):
@@ -392,7 +392,7 @@
     def group(g, half=None):
         if half is None:
             return pl.ds(pl.multiple_of(g * Z_ROWS, Z_ROWS), Z_ROWS)
-        first = 3 * CHUNK_ROWS
+        first = Z_ROWS // 2
         if half == 0:
             return pl.ds(pl.multiple_of(g * Z_ROWS, CHUNK_ROWS), first)
         return pl.ds(pl.multiple_of(g * Z_ROWS + first, CHUNK_ROWS), Z_ROWS - first)
@@ -440,10 +440,9 @@
             gate = jnp.minimum(jnp.dot(rows, gate_ref[...], preferred_element_type=F32), CLAMP)
             lift = jnp.clip(jnp.dot(rows, up_ref[...], preferred_element_type=F32), -CLAMP, CLAMP)
             active = gate * jax.nn.sigmoid(ALPHA * gate) * (lift + 1.0)
-            filler = jnp.zeros((ACT_ROWS - 24, FF_BLOCK), F32)
             for s in range(4):
-                own_rows = jnp.concatenate([active[24 * s : 24 * s + 24], filler], axis=0)
-                act_out[g, s] = own_rows.astype(BF16)
+                mine = active[OWN_ROWS * s : OWN_ROWS * s + OWN_ROWS]
+                act_out[g, s] = jnp.concatenate([mine[:, :128], mine[:, 128:]], axis=0).astype(BF16)
             act_in[g, x] = act_out[g, x]
             for n, other in enumerate((after, before, across)):
                 send(act_out.at[g, other], act_in.at[g, x], g_send, g_recv.at[n, g], {"tp": other})
@@ -461,7 +460,13 @@
 
             for n, origin in enumerate((before, after, across)):
                 await_(act_in.at[g, origin], g_recv.at[n, g])
-            acts = jnp.concatenate([act_in[g, s] for s in range(4)], axis=1)
+            lanes = []
+            for s in range(4):
+                wide = act_in[g, s].astype(F32)
+                lanes += [wide[:OWN_ROWS], wide[OWN_ROWS:]]
+            acts = jnp.concatenate(lanes, axis=1)
+            filler = jnp.zeros((32 - OWN_ROWS, 4 * FF_BLOCK), F32)
+            acts = jnp.concatenate([acts, filler], axis=0).astype(BF16)
             down = down_ref[...].reshape(4 * FF_BLOCK, WIDTH)
             result = jnp.dot(acts, down, preferred_element_type=F32).astype(BF16)
             back[group(g)] = to_chunks(result, swap_ref[...])[:Z_ROWS]
@@ -537,8 +542,8 @@
             pltpu.VMEM((TOK, WIDTH), BF16),
             pltpu.VMEM((ALL_ROWS, 128), BF16),
             pltpu.VMEM((4, ALL_ROWS, 128), BF16),
-            pltpu.VMEM((NZ, 4, ACT_ROWS, FF_BLOCK), BF16),
-            pltpu.VMEM((NZ, 4, ACT_ROWS, FF_BLOCK), BF16),
+            pltpu.VMEM((NZ, 4, 2 * OWN_ROWS, 128), BF16),
+            pltpu.VMEM((NZ, 4, 2 * OWN_ROWS, 128), BF16),
             pltpu.VMEM((ALL_ROWS, 128), BF16),
             pltpu.VMEM((ALL_ROWS, 128), BF16),
             pltpu.VMEM((256, 256), BF16),

time: 95.4 us -> 93.6 us (0.981)
  Pallas kernels: 93.5 us -> 91.7 us
    pallas_call x1, Pallas kernels: 93.5 us -> 91.7 us  [layer(): pl.pallas_call(layer_kernel, out_shape=jax.ShapeDtypeStruct(res.shape[1:]...]
where the time goes in v5:
time: 93.6 us; the launch traced here: 93.5 us
  Pallas kernels  91.7 us (98%)
  local copies, waits for them, and re-layouts  1.77 us (2%)
    pallas_call x1, Pallas kernels, layer(): pl.pallas_call(layer_kernel, out_shape=jax.ShapeDtypeStruct(res.shape[1:]...  91.7 us

profile of v5, /device:TPU:1, one launch (start us, length us, event | category | flops | bytes accessed | tf_op | source)
XLA Modules:
  0.0 93.5 jit_solution(12272298923617353153)
XLA Ops:
  0.0 91.7 %shard_map.154 = bf16[96,2048]{1,0:T(8,128)(2,1)} custom-call(f32[1,128]{1,0:T(1,128)} %bitcast.13, f32[1,2048]{1,0:T(1,128)} %bitcast.9, f32[1,128]{1,0:T(1,128)} %constant.13.inv_hbm, s32[4,2,96]{2,1,0:T(2,128)} %bitcast.11, f32[2,96]{1,0:T(2,128)} %bitcast.12, bf16[1,96,2048]{2,1,0:T(8,128)(2,1)} %res_hbm.1, bf16[1,96,1024]{2,1,0:T(8,128)(2,1)} %qn_hbm.1, ...), custom_call_target="tpu_custom_call" | custom-call | tf_op jit(solution)/shard_map/pallas_call | solution.py:525
  91.7 1.8 %copy.18 = bf16[1,96,2048]{2,1,0:T(8,128)(2,1)} copy(bf16[1,96,2048]{2,1,0:T(8,128)(2,1)} %bitcast.8) | data formatting | bytes 786432
